TPU v7x, 128 devices: a whole 4x4x4 slice. The times are simulated.
128 devices in a mesh: ep: 128 (over z, y, x, core).
Axes of the slice: x: 4, y: 4, z: 4, core: 2. Of those that a mesh axis runs over, the one named last changes fastest.
Arguments:
- tokens: bfloat16 [2048, 2048], P('ep'), may hold values from -6 to 6
- cache_keys: bfloat16 [2048, 1024, 128], P('ep'), may hold values from -6 to 6
- cache_values: bfloat16 [2048, 1024, 128], P('ep'), may hold values from -6 to 6
- cache_len: int32 [2048], P('ep'), may hold values from 1 to 1024
- norm_gain_first: float32 [2048], replicated, may hold values from 0.1 to 1.9
- w_query: bfloat16 [2048, 2048], P(None, 'ep'), may hold values from -0.125 to 0.125
- w_key: bfloat16 [2048, 128], replicated, may hold values from -0.125 to 0.125
- w_value: bfloat16 [2048, 128], replicated, may hold values from -0.125 to 0.125
- head_bias: float32 [32], replicated, may hold values from -8.5 to -3
- w_output: bfloat16 [2048, 2048], P(None, 'ep'), may hold values from -0.125 to 0.125
- norm_gain_second: float32 [2048], replicated, may hold values from 0.1 to 1.9
- group_id: int32 [2048], P('ep'), may hold values from 0 to 7, as said below
- member: int32 [2048, 6], P('ep'), may hold values from 0 to 15, as said below
- group_gate: float32 [2048], P('ep'), may hold values from 0.3 to 1
- member_weight: float32 [2048, 6], P('ep'), may hold values from 0.05 to 0.5
- expert_gate_w: bfloat16 [128, 2048, 512], P('ep'), may hold values from -0.125 to 0.125
- expert_up_w: bfloat16 [128, 2048, 512], P('ep'), may hold values from -0.125 to 0.125
- expert_down_w: bfloat16 [128, 512, 2048], P('ep'), may hold values from -0.25 to 0.25
- dense_gate_w: bfloat16 [2048, 2048], P(None, 'ep'), may hold values from -0.125 to 0.125
- dense_up_w: bfloat16 [2048, 2048], P(None, 'ep'), may hold values from -1 to 1
- hidden_gain: float32 [2048], replicated, may hold values from 0.1 to 1.9
- dense_down_w: bfloat16 [2048, 2048], P(None, 'ep'), may hold values from -0.125 to 0.125
- branch_logit: float32 [2048], replicated, may hold values from -8 to 8
Outputs:
- mixed_out: bfloat16 [2048, 2048], P('ep')
- new_keys: bfloat16 [2048, 128], P('ep')
- new_values: bfloat16 [2048, 128], P('ep')
Inputs may be any that keep to these rules, and one draw needn't show every extreme that they name: `group_id`: each group number is named by exactly 2 of the tokens of one device. `member`: each row names 6 different members; with group_id, no expert is named by more than 2 tokens of one device, and some expert is named by 2 tokens of every device.
All inputs are finite; a program needn't handle non-finite values.
Results may differ from a plain program's by a relative error of at most 0.0085.
Values may be sent and summed in bfloat16 or wider, within the bound.
A program may use at most 128 MiB of HBM per device.

v0:
```python
import jax
import jax.numpy as jnp
from jax import lax
from jax.sharding import PartitionSpec as P

D = 2048
HEADS = 32
HEAD_DIM = 64
KV_HEADS = 2
PER_GROUP = 16
TOP_K = 6


epsilon = 1e-06


def grouped_exchange(shard, axis, split_dim, concat_dim, work, item_dim, out_dim):

    def moved(group):
        return lax.all_to_all(group, axis, split_axis=split_dim, concat_axis=concat_dim, tiled=True)

    items = jax.tree.leaves(shard)[0].shape[item_dim]
    ends = [items * k // 2 for k in range(2 + 1)] if items % 2 == 0 else [0, items]
    groups = [
        jax.tree.map(lambda a: lax.slice_in_dim(a, low, high, axis=item_dim), shard)
        for low, high in zip(ends, ends[1:])
    ]
    arrived = [moved(group) for group in groups]
    made = [work(group) for group in arrived]
    return jax.tree.map(lambda *parts: jnp.concatenate(parts, axis=out_dim), *made)


def rms_scale(values):
    return lax.rsqrt(jnp.mean(values * values, axis=-1, keepdims=True) + epsilon)


def later_sum(log_remain):
    span_len = log_remain.shape[-1]
    block_len = min(128, span_len)
    block_count = span_len // block_len
    lead = log_remain.shape[:-1]
    blocked = log_remain.reshape(lead + (block_count, block_len))
    inner = jnp.arange(block_len, dtype=jnp.int32)
    inner_after = (inner[:, None] > inner[None, :]).astype(jnp.float32)
    within = jnp.einsum("abcnj,js->abcns", blocked, inner_after, precision=lax.Precision.HIGHEST)
    totals = jnp.sum(blocked, axis=-1)
    outer = jnp.arange(block_count, dtype=jnp.int32)
    outer_after = (outer[:, None] > outer[None, :]).astype(jnp.float32)
    carried = jnp.einsum("abcj,jn->abcn", totals, outer_after, precision=lax.Precision.HIGHEST)
    return (within + carried[..., None]).reshape(lead + (span_len,))


def stick_read(queries, key_cache, value_cache, lengths, head_bias):
    batch_size = queries.shape[0]
    span_len = key_cache.shape[1]
    group_size = HEADS // KV_HEADS
    query_heads = queries.reshape(batch_size, KV_HEADS, group_size, HEAD_DIM)
    key_heads = key_cache.reshape(batch_size, span_len, KV_HEADS, HEAD_DIM)
    value_heads = value_cache.reshape(batch_size, span_len, KV_HEADS, HEAD_DIM)
    scores = jnp.einsum(
        "bkgd,bskd->bkgs", query_heads, key_heads, preferred_element_type=jnp.float32
    ) * HEAD_DIM ** (-0.5)
    scores = scores + head_bias.reshape(KV_HEADS, group_size)[None, :, :, None]
    live_mask = (jnp.arange(span_len, dtype=jnp.int32)[None, :] < lengths[:, None])[
        :, None, None, :
    ]
    log_remain = jnp.where(live_mask, jax.nn.log_sigmoid(-scores), 0.0)
    remain_after = later_sum(log_remain)
    weights = jnp.where(live_mask, jnp.exp(jax.nn.log_sigmoid(scores) + remain_after), 0.0).astype(
        jnp.bfloat16
    )
    mixed_heads = jnp.einsum(
        "bkgs,bskd->bkgd", weights, value_heads, preferred_element_type=jnp.float32
    )
    return mixed_heads.reshape(batch_size, HEADS * HEAD_DIM).astype(jnp.bfloat16)


def expert_apply(flat_rows, gate_w, up_w, down_w):
    gate_pre = jnp.dot(flat_rows, gate_w, preferred_element_type=jnp.float32)
    upper_pre = jnp.dot(flat_rows, up_w, preferred_element_type=jnp.float32)
    hidden = (jax.nn.silu(gate_pre) * upper_pre).astype(jnp.bfloat16)
    return jnp.dot(hidden, down_w, preferred_element_type=jnp.float32).astype(jnp.bfloat16)


def shards(
    tokens,
    cache_keys,
    cache_values,
    cache_len,
    norm_gain_first,
    w_query,
    w_key,
    w_value,
    head_bias,
    w_output,
    norm_gain_second,
    group_id,
    member,
    group_gate,
    member_weight,
    expert_gate_w,
    expert_up_w,
    expert_down_w,
    dense_gate_w,
    dense_up_w,
    hidden_gain,
    dense_down_w,
    branch_logit,
):
    devices = lax.axis_size("ep")
    seq_dev = tokens.shape[0]
    stream = tokens.astype(jnp.float32)
    normed_first = (stream * rms_scale(stream) * norm_gain_first).astype(jnp.bfloat16)
    new_keys = jnp.dot(normed_first, w_key, preferred_element_type=jnp.float32).astype(jnp.bfloat16)
    new_values = jnp.dot(normed_first, w_value, preferred_element_type=jnp.float32).astype(
        jnp.bfloat16
    )
    queries = jnp.dot(
        normed_first,
        lax.all_gather(w_query, "ep", axis=1, tiled=True),
        preferred_element_type=jnp.float32,
    ).astype(jnp.bfloat16)
    attended = stick_read(queries, cache_keys, cache_values, cache_len, head_bias)
    projected = jnp.dot(
        attended,
        lax.all_gather(w_output, "ep", axis=1, tiled=True),
        preferred_element_type=jnp.float32,
    ).astype(jnp.bfloat16)
    second_stream = stream + projected.astype(jnp.float32)
    normed_second = (second_stream * rms_scale(second_stream) * norm_gain_second).astype(
        jnp.bfloat16
    )
    experts = devices * expert_gate_w.shape[0]
    capacity = seq_dev // (experts // PER_GROUP)
    pair_expert = (group_id[:, None] * PER_GROUP + member).reshape(-1)
    pair_count = pair_expert.shape[0]
    expert_hits = (pair_expert[:, None] == jnp.arange(experts, dtype=jnp.int32)[None, :]).astype(
        jnp.float32
    )
    earlier = (jnp.arange(pair_count)[:, None] > jnp.arange(pair_count)[None, :]).astype(
        jnp.float32
    )
    before = jnp.dot(earlier, expert_hits, preferred_element_type=jnp.float32)
    slot_index = jnp.sum(before * expert_hits, axis=1).astype(jnp.int32)
    target = pair_expert * capacity + slot_index
    select = (jnp.arange(experts * capacity, dtype=jnp.int32)[:, None] == target[None, :]).astype(
        jnp.bfloat16
    )
    pair_rows = jnp.repeat(normed_second, TOP_K, axis=0)
    packed = jnp.dot(select, pair_rows, preferred_element_type=jnp.float32).astype(jnp.bfloat16)
    packed = packed.reshape(experts, capacity, D)

    def serve(received):
        flat_rows = received.reshape(-1, received.shape[-1])
        result_rows = expert_apply(flat_rows, expert_gate_w[0], expert_up_w[0], expert_down_w[0])
        return result_rows.reshape(received.shape)

    served = grouped_exchange(packed, "ep", 0, 0, serve, 1, 1)
    returned = lax.all_to_all(served, "ep", split_axis=0, concat_axis=0, tiled=True).reshape(
        experts * capacity, D
    )
    pair_out = lax.dot_general(
        select, returned, (((0,), (0,)), ((), ())), preferred_element_type=jnp.float32
    )
    combine = (group_gate[:, None] * member_weight).reshape(-1, 1)
    routed = jnp.sum((pair_out * combine).reshape(seq_dev, TOP_K, D), axis=1)
    gathered = lax.all_gather(normed_second, "ep", axis=0, tiled=True)
    dense_gate = jnp.dot(gathered, dense_gate_w, preferred_element_type=jnp.float32)
    dense_upper = jnp.dot(gathered, dense_up_w, preferred_element_type=jnp.float32)
    dense_hidden = jax.nn.silu(dense_gate) * dense_upper
    own_hidden = lax.all_to_all(
        dense_hidden.astype(jnp.bfloat16), "ep", split_axis=0, concat_axis=1, tiled=True
    ).astype(dense_hidden.dtype)
    dense_normed = (own_hidden * rms_scale(own_hidden) * hidden_gain).astype(jnp.bfloat16)
    dense_out = jnp.dot(
        dense_normed,
        lax.all_gather(dense_down_w, "ep", axis=1, tiled=True),
        preferred_element_type=jnp.float32,
    ).astype(jnp.bfloat16)
    mixed_out = (
        second_stream + routed + jax.nn.sigmoid(branch_logit) * dense_out.astype(jnp.float32)
    )
    return (mixed_out.astype(jnp.bfloat16), new_keys, new_values)


def solution(mesh):
    in_specs = (
        P("ep", None),
        P("ep", None, None),
        P("ep", None, None),
        P("ep"),
        P(),
        P(None, "ep"),
        P(),
        P(),
        P(),
        P(None, "ep"),
        P(),
        P("ep"),
        P("ep", None),
        P("ep"),
        P("ep", None),
        P("ep", None, None),
        P("ep", None, None),
        P("ep", None, None),
        P(None, "ep"),
        P(None, "ep"),
        P(),
        P(None, "ep"),
        P(),
    )
    out_specs = (P("ep", None), P("ep", None), P("ep", None))
    return jax.shard_map(shards, mesh=mesh, in_specs=in_specs, out_specs=out_specs, check_vma=False)
```

profile of v0, /device:TPU:0, one launch (start us, length us, event | category | flops | bytes accessed | tf_op | source)
XLA Modules:
  0.0 315.0 jit_solution(9604924944444672281)
XLA Ops:
  9.4 6.4 %copy.40 = bf16[16,1024,128]{1,2,0:T(8,128)(2,1)} copy(bf16[16,1024,128]{2,1,0:T(8,128)(2,1)} %param.24) | data formatting | bytes 8388608 | tf_op args[1]
  15.9 6.4 %copy.43 = bf16[16,1024,128]{1,2,0:T(8,128)(2,1)} copy(bf16[16,1024,128]{2,1,0:T(8,128)(2,1)} %param.25) | data formatting | bytes 8388608 | tf_op args[2]
  22.6 60.6 %all-gather.5.cloned.1.call-done = bf16[2048,2048]{0,1:T(8,128)(2,1)} async-done(((bf16[2048,16]{0,1:T(8,128)(2,1)}), bf16[2048,2048]{0,1:T(8,128)(2,1)}) %all-gather.5.cloned.1.call-update) | async-done | bytes 8388624 | tf_op jit(solution)/shard_map/all_gather | solution.py:120
  83.2 5.7 %convolution_convert_fusion.5 = bf16[16,2048]{1,0:T(8,128)(2,1)S(1)} fusion(bf16[2048,2048]{0,1:T(8,128)(2,1)} %all-gather.5.cloned.1.call-done, bf16[16,2048]{1,0:T(8,128)(2,1)S(1)} %copy-done.5, f32[2048]{0:T(1024)S(1)} %copy-done.8, f32[16]{0:T(128)S(1)} %add_rsqrt_fusion.2), kind=kOutput, calls=%fused_computation.18 | convolution fusion | flops 134381568 | bytes 8527936 | tf_op jit(solution)/shard_map/dot_general | solution.py:118
  89.0 5.1 %fusion.15 = (f32[16,2,16,1024]{3,2,1,0:T(8,128)S(1)}, f32[16,2,16,1024]{3,2,1,0:T(8,128)}) fusion(f32[2,16]{1,0:T(2,128)S(1)} %add.92, pred[16,1024]{1,0:T(8,128)(4,1)S(1)} %iota_compare_fusion.4, bf16[16,2,16,64]{3,2,1,0:T(8,128)(2,1)S(1)} %reshape.117, bf16[16,1024,2,64]{1,3,2,0:T(8,128)(2,1)} %bitcast.96), kind=kOutput, calls=%fused_computation.25 | convolution fusion | flops 72351744 | bytes 8470656 | tf_op jit(solution)/shard_map/bkgd,bskd->bkgs/dot_general | solution.py:60
  98.4 4.1 %convolution_add_fusion = f32[16,2,16,8,128]{4,3,2,1,0:T(8,128)} fusion(f32[16,2,16,8,128]{4,3,2,1,0:T(8,128)} %bitcast.93, f32[16,2,16,8]{3,2,1,0:T(8,128)S(1)} %fusion.82), kind=kOutput, calls=%fused_computation.37 | convolution fusion | flops 805847040 | bytes 4210688 | tf_op jit(solution)/shard_map/abcnj,js->abcns/dot_general | solution.py:45
  102.5 2.7 reshape.120
  105.2 5.4 %convolution_convert_fusion.6 = bf16[16,2,16,64]{3,2,1,0:T(8,128)(2,1)S(1)} fusion(bf16[16,1024,2,64]{1,3,2,0:T(8,128)(2,1)} %bitcast.95, f32[16,2,16,1024]{3,2,1,0:T(8,128)} %reshape.120, f32[16,2,16,1024]{3,2,1,0:T(8,128)} %get-tuple-element.6, f32[2,16]{1,0:T(2,128)S(1)} %add.92, pred[16,1024]{1,0:T(8,128)(4,1)S(1)} %iota_compare_fusion.4), kind=kOutput, calls=%fused_computation.42 | convolution fusion | flops 73957376 | bytes 8470656 | tf_op jit(solution)/shard_map/bkgs,bskd->bkgd/dot_general | solution.py:72
  110.9 42.5 %all-gather.7.cloned.1.call-done = bf16[2048,2048]{0,1:T(8,128)(2,1)} async-done(((bf16[2048,16]{0,1:T(8,128)(2,1)}), bf16[2048,2048]{0,1:T(8,128)(2,1)}) %all-gather.7.cloned.1.call-update) | async-done | bytes 8388624 | tf_op jit(solution)/shard_map/all_gather | solution.py:126
  153.4 5.8 %multiply_reduce_fusion.1 = (f32[16]{0:T(128)S(1)}, f32[16,2048]{1,0:T(8,128)S(1)}) fusion(bf16[16,2048]{1,0:T(8,128)(2,1)S(1)} %convert_element_type.93, bf16[2048,2048]{0,1:T(8,128)(2,1)} %all-gather.7.cloned.1.call-done, bf16[16,2048]{1,0:T(8,128)(2,1)S(1)} %copy-done.5), kind=kOutput, calls=%fused_computation.79 | convolution fusion | flops 134414320 | bytes 8650816 | tf_op jit(solution)/shard_map/dot_general | solution.py:124
  165.2 2.5 fusion.91
  168.2 5.6 %reduce.3 = bf16[128,2048]{1,0:T(8,128)(2,1)} reduce(bf16[128,1,2048]{2,1,0:T(2,128)(2,1)} %get-tuple-element.3, bf16[]{:T(256)} %broadcast.88), dimensions={1}, to_apply=%get-tuple-element.3.reduce_sub_computation | reduce | bytes 1048578 | tf_op jit(solution)/shard_map/slice | solution.py:25
  176.0 6.7 %all-to-all-start = ((bf16[128,2,1024]{2,1,0:T(2,128)(2,1)}), bf16[128,2,1024]{2,1,0:T(2,128)(2,1)}, u32[]{:S(2)}, u32[]{:S(2)}) async-start(bf16[128,2,1024]{2,1,0:T(2,128)(2,1)} %reshape.136), calls=%async_computation | async-start | bytes 1048576 | tf_op jit(solution)/shard_map/all_to_all | solution.py:20
  182.7 4.5 %reduce.2 = bf16[128,2048]{1,0:T(8,128)(2,1)} reduce(bf16[128,1,2048]{2,1,0:T(2,128)(2,1)S(1)} %copy-done.3, bf16[]{:T(256)} %broadcast.88), dimensions={1}, to_apply=%get-tuple-element.4.reduce_sub_computation | reduce | bytes 1048578 | tf_op jit(solution)/shard_map/slice | solution.py:25
  187.2 2.2 reshape.134
  189.4 6.3 %all-to-all-done = bf16[128,2,1024]{2,1,0:T(2,128)(2,1)} async-done(((bf16[128,2,1024]{2,1,0:T(2,128)(2,1)}), bf16[128,2,1024]{2,1,0:T(2,128)(2,1)}, u32[]{:S(2)}, u32[]{:S(2)}) %all-to-all-start) | async-done | bytes 524320 | tf_op jit(solution)/shard_map/all_to_all | solution.py:20
  195.8 6.0 %all-to-all-start.1 = ((bf16[128,2,1024]{2,1,0:T(2,128)(2,1)}), bf16[128,2,1024]{2,1,0:T(2,128)(2,1)}, u32[]{:S(2)}, u32[]{:S(2)}) async-start(bf16[128,2,1024]{2,1,0:T(2,128)(2,1)} %reshape.134), calls=%async_computation.1 | async-start | bytes 1048576 | tf_op jit(solution)/shard_map/all_to_all | solution.py:20
  201.7 3.6 %reshape.137 = bf16[128,1,2048]{2,1,0:T(2,128)(2,1)S(1)} reshape(bf16[128,2,1024]{2,1,0:T(2,128)(2,1)} %all-to-all-done) | data formatting | bytes 1048576
  205.3 9.3 %all-to-all-done.1 = bf16[128,2,1024]{2,1,0:T(2,128)(2,1)} async-done(((bf16[128,2,1024]{2,1,0:T(2,128)(2,1)}), bf16[128,2,1024]{2,1,0:T(2,128)(2,1)}, u32[]{:S(2)}, u32[]{:S(2)}) %all-to-all-start.1) | async-done | bytes 524320 | tf_op jit(solution)/shard_map/all_to_all | solution.py:20
  214.6 4.3 %reshape.135 = bf16[128,1,2048]{2,1,0:T(2,128)(2,1)} reshape(bf16[128,2,1024]{2,1,0:T(2,128)(2,1)} %all-to-all-done.1) | data formatting | bytes 1048576
  218.9 3.1 fusion.24
  222.0 2.4 fusion.22
  224.5 3.4 %fusion = bf16[128,1,2048]{2,0,1:T(8,128)(2,1)} fusion(bf16[1,512,2048]{2,1,0:T(8,128)(2,1)S(1)} %copy-done, bf16[1,2048,512]{2,1,0:T(8,128)(2,1)} %param.39, f32[128,512]{1,0:T(8,128)} %fusion.24, bf16[128,1,2048]{2,1,0:T(2,128)(2,1)S(1)} %reshape.137), kind=kOutput, calls=%fused_computation.6 | convolution fusion | flops 537526272 | bytes 5505024 | tf_op jit(solution)/shard_map/dot_general | solution.py:82
  227.9 2.9 fusion.1
  233.0 5.8 %all-to-all-start.2 = ((bf16[128,2,2048]{2,1,0:T(2,128)(2,1)}), bf16[128,2,2048]{2,1,0:T(2,128)(2,1)}, u32[]{:S(2)}, u32[]{:S(2)}) async-start(bf16[128,2,2048]{2,1,0:T(2,128)(2,1)} %copy.45), calls=%async_computation.2 | async-start | bytes 2097152 | tf_op jit(solution)/shard_map/all_to_all | solution.py:159
  240.7 17.5 %all-to-all-done.2 = bf16[128,2,2048]{2,1,0:T(2,128)(2,1)} async-done(((bf16[128,2,2048]{2,1,0:T(2,128)(2,1)}), bf16[128,2,2048]{2,1,0:T(2,128)(2,1)}, u32[]{:S(2)}, u32[]{:S(2)}) %all-to-all-start.2) | async-done | bytes 1048608 | tf_op jit(solution)/shard_map/all_to_all | solution.py:159
  259.7 5.8 %fusion.92 = f32[2048,16]{0,1:T(8,128)S(1)} fusion(bf16[2048,2048]{1,0:T(8,128)(2,1)} %all-gather.9.cloned.1.call-done, bf16[2048,16]{0,1:T(8,128)(2,1)S(1)} %copy-done.9), kind=kOutput, calls=%fused_computation.109 | convolution fusion | flops 134217728 | bytes 8585216 | tf_op jit(solution)/shard_map/dot_general | solution.py:168
  265.6 2.3 fusion.2
  273.4 4.8 %all-to-all-start.3 = ((bf16[128,2,128]{2,1,0:T(2,128)(2,1)}), bf16[128,2,128]{2,1,0:T(2,128)(2,1)S(1)}, u32[]{:S(2)}, u32[]{:S(2)}) async-start(bf16[128,2,128]{2,1,0:T(2,128)(2,1)} %reshape.138), calls=%async_computation.3 | async-start | bytes 131072 | tf_op jit(solution)/shard_map/all_to_all | solution.py:171
  281.1 6.1 %all-to-all-done.3 = bf16[128,2,128]{2,1,0:T(2,128)(2,1)S(1)} async-done(((bf16[128,2,128]{2,1,0:T(2,128)(2,1)}), bf16[128,2,128]{2,1,0:T(2,128)(2,1)S(1)}, u32[]{:S(2)}, u32[]{:S(2)}) %all-to-all-start.3) | async-done | bytes 65568 | tf_op jit(solution)/shard_map/all_to_all | solution.py:171
  290.6 11.5 %all-gather.11.cloned.1.call-done = bf16[2048,2048]{0,1:T(8,128)(2,1)} async-done(((bf16[2048,16]{0,1:T(8,128)(2,1)}), bf16[2048,2048]{0,1:T(8,128)(2,1)}) %all-gather.11.cloned.1.call-update) | async-done | bytes 8388624 | tf_op jit(solution)/shard_map/all_gather | solution.py:177
  302.1 6.3 %fusion.6 = bf16[16,2048]{1,0:T(8,128)(2,1)} fusion(bf16[2048,2048]{0,1:T(8,128)(2,1)} %all-gather.11.cloned.1.call-done, f32[16,2048]{1,0:T(8,128)S(1)} %get-tuple-element.8, f32[16,2048]{1,0:T(8,128)S(1)} %reduce_sum.58, f32[16,2048]{1,0:T(8,128)S(1)} %copy.53, f32[2048]{0:T(1024)S(1)} %copy-done.11, f32[16]{0:T(128)S(1)} %add_rsqrt_fusion, ...), kind=kOutput, calls=%fused_computation.14 | convolution fusion | flops 134512640 | bytes 8863808 | tf_op jit(solution)/shard_map/dot_general | solution.py:175
  (90 shorter events, 33.2 us)
Async XLA Ops:
  7.2 217.3 %copy-start = (bf16[1,512,2048]{2,1,0:T(8,128)(2,1)S(1)}, bf16[1,512,2048]{2,1,0:T(8,128)(2,1)}, u32[]{:S(2)}) copy-start(bf16[1,512,2048]{2,1,0:T(8,128)(2,1)} %param.40) | copy-start | bytes 6291460
  7.2 76.0 %all-gather.5.cloned.1.call-start = ((), (), s32[]{:S(2)}) async-start(), calls=%async_computation.4 | async-start | bytes 8454144 | tf_op jit(solution)/shard_map/all_gather | solution.py:120
  7.9 145.5 %all-gather.7.cloned.1.call-start = ((), (), s32[]{:S(2)}) async-start(), calls=%async_computation.5 | async-start | bytes 8454144 | tf_op jit(solution)/shard_map/all_gather | solution.py:126
  8.7 251.0 %all-gather.9.cloned.1.call-start = ((), (), s32[]{:S(2)}) async-start(), calls=%async_computation.6 | async-start | bytes 8454144 | tf_op jit(solution)/shard_map/all_gather | solution.py:167
  15.9 6.4 %copy-start.5 = (bf16[16,2048]{1,0:T(8,128)(2,1)S(1)}, bf16[16,2048]{1,0:T(8,128)(2,1)}, u32[]{:S(2)}) copy-start(bf16[16,2048]{1,0:T(8,128)(2,1)} %param.23) | copy-start | bytes 196612
  15.9 6.6 %copy-start.16 = (s32[16]{0:T(128)S(1)}, s32[16]{0:T(128)}, u32[]{:S(2)}) copy-start(s32[16]{0:T(128)} %param.26) | copy-start | bytes 196
  15.9 67.3 %copy-start.8 = (f32[2048]{0:T(1024)S(1)}, f32[2048]{0:T(1024)}, u32[]{:S(2)}) copy-start(f32[2048]{0:T(1024)} %param.27) | copy-start | bytes 24580
  110.9 48.3 %copy-start.12 = (f32[2048]{0:T(1024)S(1)}, f32[2048]{0:T(1024)}, u32[]{:S(2)}) copy-start(f32[2048]{0:T(1024)} %param.33) | copy-start | bytes 24580
  110.9 49.6 %copy-start.18 = (s32[16]{0:T(128)S(1)}, s32[16]{0:T(128)}, u32[]{:S(2)}) copy-start(s32[16]{0:T(128)} %param.34) | copy-start | bytes 196
  110.9 49.6 %copy-start.14 = (s32[16,6]{0,1:T(8,128)S(1)}, s32[16,6]{0,1:T(8,128)}, u32[]{:S(2)}) copy-start(s32[16,6]{0,1:T(8,128)} %param.35) | copy-start | bytes 1156
  159.9 142.2 %all-gather.11.cloned.1.call-start = ((), (), s32[]{:S(2)}) async-start(), calls=%async_computation.7 | async-start | bytes 8454144 | tf_op jit(solution)/shard_map/all_gather | solution.py:177
  167.7 15.0 %copy-start.3 = (bf16[128,1,2048]{2,1,0:T(2,128)(2,1)S(1)}, bf16[128,1,2048]{2,1,0:T(2,128)(2,1)}, u32[]{:S(2)}) copy-start(bf16[128,1,2048]{2,1,0:T(2,128)(2,1)} %get-tuple-element.4) | copy-start | bytes 1572868
  176.0 19.8 %all-to-all-start = ((bf16[128,2,1024]{2,1,0:T(2,128)(2,1)}), bf16[128,2,1024]{2,1,0:T(2,128)(2,1)}, u32[]{:S(2)}, u32[]{:S(2)}) async-start(bf16[128,2,1024]{2,1,0:T(2,128)(2,1)} %reshape.136), calls=%async_computation | async-start | bytes 1048576 | tf_op jit(solution)/shard_map/all_to_all | solution.py:20
  195.8 18.8 %all-to-all-start.1 = ((bf16[128,2,1024]{2,1,0:T(2,128)(2,1)}), bf16[128,2,1024]{2,1,0:T(2,128)(2,1)}, u32[]{:S(2)}, u32[]{:S(2)}) async-start(bf16[128,2,1024]{2,1,0:T(2,128)(2,1)} %reshape.134), calls=%async_computation.1 | async-start | bytes 1048576 | tf_op jit(solution)/shard_map/all_to_all | solution.py:20
  218.9 3.1 copy-start.2
  227.9 2.9 copy-start.4
  230.9 7.9 %copy-start.15 = (f32[16,6]{0,1:T(8,128)S(1)}, f32[16,6]{0,1:T(8,128)}, u32[]{:S(2)}) copy-start(f32[16,6]{0,1:T(8,128)} %param.37) | copy-start | bytes 1156
  230.9 7.9 %copy-start.17 = (f32[16]{0:T(128)S(1)}, f32[16]{0:T(128)}, u32[]{:S(2)}) copy-start(f32[16]{0:T(128)} %param.36) | copy-start | bytes 196
  230.9 8.1 %copy-start.13 = (f32[2048]{0:T(1024)S(1)}, f32[2048]{0:T(1024)}, u32[]{:S(2)}) copy-start(f32[2048]{0:T(1024)} %param.45) | copy-start | bytes 24580
  230.9 8.1 %copy-start.6 = (bf16[2048,128]{1,0:T(8,128)(2,1)S(1)}, bf16[2048,128]{1,0:T(8,128)(2,1)}, u32[]{:S(2)}) copy-start(bf16[2048,128]{1,0:T(8,128)(2,1)} %param.30) | copy-start | bytes 1572868
  230.9 9.0 %copy-start.7 = (bf16[2048,128]{1,0:T(8,128)(2,1)S(1)}, bf16[2048,128]{1,0:T(8,128)(2,1)}, u32[]{:S(2)}) copy-start(bf16[2048,128]{1,0:T(8,128)(2,1)} %param.29) | copy-start | bytes 1572868
  233.0 25.2 %all-to-all-start.2 = ((bf16[128,2,2048]{2,1,0:T(2,128)(2,1)}), bf16[128,2,2048]{2,1,0:T(2,128)(2,1)}, u32[]{:S(2)}, u32[]{:S(2)}) async-start(bf16[128,2,2048]{2,1,0:T(2,128)(2,1)} %copy.45), calls=%async_computation.2 | async-start | bytes 2097152 | tf_op jit(solution)/shard_map/all_to_all | solution.py:159
  238.8 20.9 %copy-start.9 = (bf16[2048,16]{0,1:T(8,128)(2,1)S(1)}, bf16[2048,16]{0,1:T(8,128)(2,1)}, u32[]{:S(2)}) copy-start(bf16[2048,16]{0,1:T(8,128)(2,1)} %param.41) | copy-start | bytes 196612
  259.7 5.9 %copy-start.10 = (bf16[2048,16]{0,1:T(8,128)(2,1)S(1)}, bf16[2048,16]{0,1:T(8,128)(2,1)}, u32[]{:S(2)}) copy-start(bf16[2048,16]{0,1:T(8,128)(2,1)} %param.42) | copy-start | bytes 196612
  259.7 5.9 %copy-start.1 = (bf16[2048,2048]{1,0:T(8,128)(2,1)S(1)}, bf16[2048,2048]{1,0:T(8,128)(2,1)}, u32[]{:S(2)}) copy-start(bf16[2048,2048]{1,0:T(8,128)(2,1)} %all-gather.9.cloned.1.call-done) | copy-start | bytes 25165828
  273.4 13.9 %all-to-all-start.3 = ((bf16[128,2,128]{2,1,0:T(2,128)(2,1)}), bf16[128,2,128]{2,1,0:T(2,128)(2,1)S(1)}, u32[]{:S(2)}, u32[]{:S(2)}) async-start(bf16[128,2,128]{2,1,0:T(2,128)(2,1)} %reshape.138), calls=%async_computation.3 | async-start | bytes 131072 | tf_op jit(solution)/shard_map/all_to_all | solution.py:171
  281.1 21.0 %copy-start.11 = (f32[2048]{0:T(1024)S(1)}, f32[2048]{0:T(1024)}, u32[]{:S(2)}) copy-start(f32[2048]{0:T(1024)} %param.43) | copy-start | bytes 24580
Sparse Core Ops, SparseCore 0:
  11.0 72.1 all-gather.4
  86.2 67.1 all-gather.6
  160.0 67.2 all-gather.8
  230.1 71.9 all-gather.10
where the time goes:
time: 318 us; the launch traced here: 315 us
  waiting for transfers between devices  156 us (49%)
  matrix products  57.2 us (18%)
  local copies, waits for them, and re-layouts  49.4 us (16%)
  starting transfers between devices  23.6 us (7%)
  other arithmetic  15.1 us (5%)
  between operations  14.2 us (4%)
    all_gather x1, waiting for transfers between devices, shards(): lax.all_gather(w_query, 'ep', axis=1, tiled=True)  60.6 us
    all_gather x1, waiting for transfers between devices, shards(): lax.all_gather(w_output, 'ep', axis=1, tiled=True)  42.5 us
    unnamed x47, local copies, waits for them, and re-layouts  29.6 us
    all_to_all x1, waiting for transfers between devices, shards(): lax.all_to_all(served, 'ep', split_axis=0, concat_axis=0, tiled=True)  17.5 us
    all_to_all x2, waiting for transfers between devices, moved(): lax.all_to_all(group, axis, split_axis=split_dim, concat_axis=concat_dim,...  15.6 us
    all_to_all x2, starting transfers between devices, moved(): lax.all_to_all(group, axis, split_axis=split_dim, concat_axis=concat_dim,...  12.6 us
    all_gather x1, waiting for transfers between devices, shards(): lax.all_gather(dense_down_w, 'ep', axis=1, tiled=True)  11.5 us
    slice x2, other arithmetic, grouped_exchange(): lax.slice_in_dim(a, low, high, axis=item_dim)  10.1 us
  transfers between devices with their start and end apart: 8, of which 7 were waited for; matrix products, arithmetic and copies ran while one was open for 34% of the time, Pallas kernels for 0%

commit v1 on v0

v1 whole, which is shorter than its diff:
```python
import functools

import jax
import jax.numpy as jnp
from jax import lax
from jax.experimental import pallas as pl
from jax.experimental.pallas import tpu as pltpu
from jax.sharding import PartitionSpec as P

D = 2048
HEADS = 32
HEAD_DIM = 64
SEQ = 16
CACHE = 1024
BLK = 256
EPS = 1e-06
F32 = jnp.float32
BF = jnp.bfloat16
MESH = pl.DeviceIdType.MESH
NT = (((1,), (1,)), ((), ()))
HI = lax.Precision.HIGHEST


def iota(shape, dim):
    return lax.broadcasted_iota(jnp.int32, shape, dim)


def one_hot(mask):
    return jnp.where(mask, 1.0, 0.0)


def dot(a, b):
    return jnp.dot(a, b, preferred_element_type=F32)


def dot_nt(a, b):
    return lax.dot_general(a, b, NT, preferred_element_type=F32)


def split2(v):
    high = v.astype(BF)
    return high, (v - high.astype(F32)).astype(BF)


def remote(src, dst, sems, target):
    return pltpu.make_async_remote_copy(
        src_ref=src,
        dst_ref=dst,
        send_sem=sems.at[0],
        recv_sem=sems.at[1],
        device_id=(target,),
        device_id_type=MESH,
    )


def take(ref, sem):
    pltpu.make_async_copy(ref, ref, sem).wait()


def lanes(k):
    return pl.ds(pl.multiple_of(k * BLK, BLK), BLK)


def kernel(
    tok, ck, cv, clen, g1, wq, wk, wv, hb, wo, g2, gid, mem, gg, mw, eg, eu, ed, wg, wu, hg, wd, bl,
    out, nk, nv,
    kb, vb, egb, eub, edb, wkb, wvb,
    wqb, wob, wgb, wub, wdb,
    xa, xc, xd, qs, qr, ts, tb, cs0, cb, cs, cd, pq, po, qstack, qb, ob, ps, pr, ys,
    sq, sqr, zb, zs, zr, hbuf,
    lsem, s_wq, s_wo, s_wg, s_wu, s_wd, s_pair, s_ex, s_xa, s_xc, s_ts, s_cb, s_cd, s_q, s_pr, s_y, s_sq, s_z,
):
    me = lax.axis_index("ep")
    chip = me // 2
    core = me % 2
    group = me // 16
    place = chip % 8
    pair = chip * 2 + (1 - core)

    local = [
        pltpu.make_async_copy(ck, kb, lsem.at[0]),
        pltpu.make_async_copy(cv, vb, lsem.at[1]),
        pltpu.make_async_copy(wk, wkb, lsem.at[2]),
        pltpu.make_async_copy(wv, wvb, lsem.at[3]),
        pltpu.make_async_copy(eg.at[0], egb.at[0], lsem.at[4]),
        pltpu.make_async_copy(eu.at[0], eub.at[0], lsem.at[5]),
        pltpu.make_async_copy(ed.at[0], edb.at[0], lsem.at[6]),
    ]

    barrier = pltpu.get_barrier_semaphore()

    def greet(k, carry):
        other = (chip + k) % 64 * 2 + core
        pl.semaphore_signal(barrier, inc=1, device_id=(other,), device_id_type=MESH)
        return carry

    pl.semaphore_signal(barrier, inc=1, device_id=(pair,), device_id_type=MESH)
    lax.fori_loop(1, 64, greet, 0)
    for c in local:
        c.start()

    x = tok[...].astype(F32)
    normed = (x * lax.rsqrt(jnp.mean(x * x, axis=-1, keepdims=True) + EPS) * g1[...]).astype(BF)
    xa[place] = normed
    gids = gid[...]
    hits = one_hot(iota((8, SEQ), 0) == gids)
    before = dot(hits, one_hot(iota((SEQ, SEQ), 0) < iota((SEQ, SEQ), 1)))
    rank = jnp.sum(hits * before, axis=0, keepdims=True).astype(jnp.int32)
    spot = gids * 2 + rank
    order = one_hot(iota((SEQ, SEQ), 0) == spot)
    eye16 = iota((SEQ, SEQ), 0) == iota((SEQ, SEQ), 1)
    spot_col = jnp.sum(jnp.where(eye16, jnp.broadcast_to(spot, (SEQ, SEQ)), 0), axis=1, keepdims=True)
    back = one_hot(iota((SEQ, SEQ), 1) == spot_col).astype(BF)
    order_bf = order.astype(BF)
    sorted_tok = dot(order_bf, tok[...]).astype(BF)
    for k in range(8):
        ts[k] = sorted_tok[:, k * BLK : (k + 1) * BLK]
    share = jnp.zeros((128, SEQ), F32)
    for k in range(6):
        share = share + jnp.where(iota((128, SEQ), 0) == mem[k : k + 1, :], mw[k : k + 1, :], 0.0)
    share = share * gg[...]
    shared = lax.dot_general(order, share, NT, precision=HI, preferred_element_type=F32)
    cs0[...] = shared
    tb[place] = ts[place]
    cb[place] = shared

    pl.semaphore_wait(barrier, 64)

    def spread_strip(strip, buf, sems):
        slot = buf.at[place, core]

        def send(k, carry):
            g = (group + k) % 8
            remote(strip, slot, sems, (g * 8 + group) * 2 + core).start()
            return carry

        @pl.when(place == group)
        def _():
            pltpu.make_async_copy(strip, slot, sems.at[1]).start()

        @pl.when(place != group)
        def _():
            send(0, 0)

        lax.fori_loop(1, 8, send, 0)

    def strip_sent(strip, buf, sems):
        take(buf.at[pl.ds(0, 7), core], sems.at[0])

        @pl.when(place != group)
        def _():
            take(buf.at[0, core], sems.at[0])

    def pass_on(buf, sems, k):
        take(buf.at[:, core], sems.at[1])
        remote(buf.at[:, core], buf.at[:, core], s_pair.at[k], pair).start()

    def in_group(src_of, dst, sems):
        def send(k, carry):
            p = (place + k) % 8
            remote(src_of(p), dst, sems, (group * 8 + p) * 2 + core).start()
            return carry

        lax.fori_loop(1, 8, send, 0)

    def over_plane(src_of, dst_of, sems):
        def send(k, carry):
            other = (chip + k) % 64
            remote(src_of(other), dst_of(other), sems, other * 2 + core).start()
            return carry

        lax.fori_loop(1, 64, send, 0)

    spread_strip(wq, wqb, s_wq)
    in_group(lambda p: xa.at[place], xa.at[place], s_xa)
    in_group(lambda p: ts.at[p], tb.at[place], s_ts)
    in_group(lambda p: cs0, cb.at[place], s_cb)

    local[2].wait()
    local[3].wait()
    nk[...] = dot(normed, wkb[...]).astype(BF)
    nv[...] = dot(normed, wvb[...]).astype(BF)
    rows, cols = iota((512, 512), 0), iota((512, 512), 1)
    pq[...] = one_hot(cols == rows % 32 * 16 + rows // 32).astype(BF)
    po[...] = one_hot(cols == rows % 16 * 32 + rows // 16).astype(BF)
    r, c = iota((128, 128), 0), iota((128, 128), 1)
    regroup = one_hot(c == r % 16 // 2 * 16 + r // 16 * 2 + r % 2)
    fold = one_hot(c == r % 8 * 16 + r // 16 * 2 + r % 16 // 8).astype(BF)
    eye = r == c
    eye32 = iota((32, 32), 0) == iota((32, 32), 1)
    bias = jnp.sum(jnp.where(eye32, jnp.broadcast_to(hb[...], (32, 32)), 0.0), axis=1, keepdims=True)
    tri = one_hot(iota((BLK, BLK), 0) >= iota((BLK, BLK), 1)).astype(BF)

    pass_on(wqb, s_wq, 0)
    take(xa.at[pl.ds(0, 7)], s_xa.at[1])
    take(wqb.at[:, core], s_pair.at[0, 1])
    q = dot_nt(xa[...].reshape(128, D), wqb[...].reshape(BLK, D)).astype(BF)
    qs[...] = q.reshape(8, SEQ, BLK)
    qr[:, lanes(place)] = qs[place]
    in_group(lambda p: qs.at[p], qr.at[:, lanes(place)], s_q)

    spread_strip(wo, wob, s_wo)
    remote(eg.at[0], egb.at[1], s_ex.at[0], pair).start()
    remote(eu.at[0], eub.at[1], s_ex.at[1], pair).start()
    remote(ed.at[0], edb.at[1], s_ex.at[2], pair).start()

    take(tb.at[pl.ds(0, 7)], s_ts.at[1])
    take(cb.at[pl.ds(0, 7)], s_cb.at[1])
    combs = jnp.dot(regroup, cb[...].reshape(128, 128), precision=HI, preferred_element_type=F32)
    cs[...] = combs.reshape(8, SEQ, 128)
    cd[group] = cs[group]

    def send_comb(k, carry):
        g = (group + k) % 8
        remote(cs.at[g], cd.at[group], s_cd, (g * 8 + place) * 2 + core).start()
        return carry

    lax.fori_loop(1, 8, send_comb, 0)

    take(qr.at[:, pl.ds(0, 7 * BLK)], s_q.at[1])
    left = iota((SEQ, 128), 1) < HEAD_DIM
    for t in range(16):
        v = qr[:, t * 128 : (t + 1) * 128].astype(F32) * HEAD_DIM**-0.5
        w = pltpu.roll(v, HEAD_DIM, 1)
        first, second = (v, w) if t < 8 else (w, v)
        keep = left if t < 8 else jnp.logical_not(left)
        qstack[32 * t : 32 * t + 16, :] = jnp.where(keep, first, 0.0).astype(BF)
        qstack[32 * t + 16 : 32 * t + 32, :] = jnp.where(keep, second, 0.0).astype(BF)
    qb[...] = dot(pq[...], qstack[...]).astype(BF).reshape(SEQ, HEADS, 128)
    local[0].wait()
    local[1].wait()
    spread_strip(wg, wgb, s_wg)
    spread_strip(wu, wub, s_wu)

    def attend(b, carry):
        s = dot_nt(qb[b], kb[b]) + bias
        live = iota((HEADS, CACHE), 1) < clen[b]
        rest = jnp.where(live, -(jnp.maximum(s, 0.0) + jnp.log(1.0 + jnp.exp(-jnp.abs(s)))), 0.0)
        high, low = split2(rest)
        parts = [v[:, n * BLK : (n + 1) * BLK] for v in (high, low) for n in range(4)]
        sums = dot(jnp.concatenate(parts, axis=0), tri)
        run = jnp.zeros((HEADS, 1), F32)
        later = []
        for n in (3, 2, 1, 0):
            within = sums[n * 32 : n * 32 + 32] + sums[128 + n * 32 : 160 + n * 32]
            later.append(within + run)
            run = run + within[:, 0:1]
        later = jnp.concatenate(later[::-1], axis=1)
        weights = jnp.where(live, jnp.exp(s + later), 0.0).astype(BF)
        ob[b] = dot(weights, vb[b]).astype(BF)
        return carry

    lax.fori_loop(0, 8, attend, 0)
    pass_on(wob, s_wo, 1)
    lax.fori_loop(8, 16, attend, 0)

    heads = dot(po[...], ob[...].reshape(512, 128))
    for t in range(16):
        a = heads[32 * t : 32 * t + 16, :]
        b = heads[32 * t + 16 : 32 * t + 32, :]
        if t < 8:
            joined = jnp.where(left, a, pltpu.roll(b, HEAD_DIM, 1))
        else:
            joined = jnp.where(left, pltpu.roll(a, HEAD_DIM, 1), b)
        xc[place, :, t * 128 : (t + 1) * 128] = dot(order_bf, joined.astype(BF)).astype(BF)
    in_group(lambda p: xc.at[place], xc.at[place], s_xc)

    over_plane(lambda o: wd.at[:, lanes(o % 8)], lambda o: wdb.at[chip, core], s_wd)
    own_wd = pltpu.make_async_copy(wd.at[:, lanes(place)], wdb.at[chip, core], lsem.at[7])
    own_wd.start()

    take(wob.at[:, core], s_pair.at[1, 1])
    take(xc.at[pl.ds(0, 7)], s_xc.at[1])
    proj = dot_nt(xc[...].reshape(128, D), wob[...].reshape(BLK, D)).astype(BF)
    stream = tb[...].reshape(128, BLK).astype(F32) + proj.astype(F32)
    y = (stream * g2[:, lanes(place)]).astype(BF)
    ys[...] = dot(regroup.astype(BF), y).astype(BF).reshape(8, SEQ, BLK)
    xd[group, :, lanes(place)] = ys[group]
    over_plane(lambda o: ys.at[o // 8], lambda o: xd.at[group, :, lanes(place)], s_y)
    ps[...] = proj.reshape(8, SEQ, BLK)
    pr[:, lanes(place)] = ps[place]
    in_group(lambda p: ps.at[p], pr.at[:, lanes(place)], s_pr)

    pass_on(wgb, s_wg, 2)
    pass_on(wub, s_wu, 3)
    own_wd.wait()
    take(wdb.at[pl.ds(0, 63), core], s_wd.at[1])
    remote(wdb.at[:, core], wdb.at[:, core], s_pair.at[4], pair).start()
    take(cd.at[pl.ds(0, 7)], s_cd.at[1])
    lane = iota((128, 128), 1)
    comb = cd[...].reshape(128, 128)
    member0 = place * 2 + core
    member1 = place * 2 + 1 - core
    comb0 = jnp.sum(jnp.where(lane == member0, comb, 0.0), axis=1, keepdims=True)
    comb1 = jnp.sum(jnp.where(lane == member1, comb, 0.0), axis=1, keepdims=True)

    take(zr.at[pl.ds(0, 63)], s_y.at[1])
    rows_in = xd[...].reshape(128, D)
    plain = rows_in.astype(F32) * (1.0 / g2[...])
    scale = lax.rsqrt(jnp.mean(plain * plain, axis=1, keepdims=True) + EPS)
    take(wgb.at[:, core], s_pair.at[2, 1])
    take(wub.at[:, core], s_pair.at[3, 1])
    gate = dot_nt(rows_in, wgb[...].reshape(BLK, D)) * scale
    upper = dot_nt(rows_in, wub[...].reshape(BLK, D)) * scale
    hidden = gate * jax.nn.sigmoid(gate) * upper
    part = jnp.sum(hidden * hidden, axis=1, keepdims=True)
    part_row = jnp.sum(jnp.where(eye, jnp.broadcast_to(part, (128, 128)), 0.0), axis=0, keepdims=True)
    sq[...] = jnp.broadcast_to(part_row, (8, 128))
    sqr[place] = sq[...]
    in_group(lambda p: sq, sqr.at[place], s_sq)

    for e, comb_e in ((0, comb0), (1, comb1)):
        if e == 0:
            for k in (4, 5, 6):
                local[k].wait()
        else:
            take(egb.at[1], s_ex.at[0, 1])
            take(eub.at[1], s_ex.at[1, 1])
            take(edb.at[1], s_ex.at[2, 1])
        gate_e = dot(rows_in, egb[e]) * scale
        upper_e = dot(rows_in, eub[e]) * scale
        hbuf[:, e * 512 : (e + 1) * 512] = (gate_e * jax.nn.sigmoid(gate_e) * upper_e * comb_e).astype(BF)

    take(sqr.at[pl.ds(0, 7)], s_sq.at[1])
    total = jnp.sum(sqr[...], axis=0)[0:1, :]
    total_col = jnp.sum(jnp.where(eye, jnp.broadcast_to(total, (128, 128)), 0.0), axis=1, keepdims=True)
    dense_scale = lax.rsqrt(total_col * (1.0 / D) + EPS)
    dense = (hidden * dense_scale * hg[:, lanes(place)]).astype(BF)
    take(wdb.at[:, core], s_pair.at[4, 1])

    def produce(k, carry):
        routed = dot(hbuf[...], edb[:, :, lanes(k)].reshape(1024, BLK))
        down = dot_nt(dense, wdb[pl.ds(k * 8, 8)].reshape(BLK, BLK))
        z = routed + jax.nn.sigmoid(bl[:, lanes(k)]) * down
        zb[k] = z.astype(BF).reshape(8, SEQ, BLK)
        return carry

    lax.fori_loop(0, 8, produce, 0)

    def give(k, carry):
        g = (group + k) % 8
        zs[g] = dot(fold, zb[:, g].reshape(128, BLK)).astype(BF).reshape(8, SEQ, BLK)

        def send(j, carry):
            p = (place + j) % 8
            remote(zs.at[g, p], zr.at[chip], s_z, (g * 8 + p) * 2 + core).start()
            return carry

        @pl.when(g == group)
        def _():
            zr[chip] = zs[g, place]

        @pl.when(g != group)
        def _():
            send(0, 0)

        lax.fori_loop(1, 8, send, 0)
        return carry

    lax.fori_loop(0, 8, give, 0)

    spots = dot_nt(one_hot(iota((128, SEQ), 0) % 16 == iota((128, SEQ), 1)), order)
    unfold = dot(spots, one_hot(iota((SEQ, 128), 1) // 8 == iota((SEQ, 128), 0)))
    unfold = jnp.where(r // 16 == c % 8, unfold, 0.0).astype(BF)
    take(pr.at[:, pl.ds(0, 7 * BLK)], s_pr.at[1])
    second = tok[...].astype(F32) + dot(back, pr[...])
    take(zr.at[pl.ds(0, 63)], s_z.at[1])
    sums = jnp.sum(zr[...].reshape(8, 8, SEQ, BLK).astype(F32), axis=1).reshape(128, BLK)
    high, low = split2(sums)
    branch = dot(unfold, high) + dot(unfold, low)
    for k in range(8):
        s = slice(k * BLK, (k + 1) * BLK)
        out[:, s] = (second[:, s] + branch[k * 16 : k * 16 + 16]).astype(BF)

    strip_sent(wq, wqb, s_wq)
    strip_sent(wo, wob, s_wo)
    strip_sent(wg, wgb, s_wg)
    strip_sent(wu, wub, s_wu)
    take(wdb.at[pl.ds(0, 63), core], s_wd.at[0])
    for k, buf in enumerate((wqb, wob, wgb, wub, wdb)):
        take(buf.at[:, core], s_pair.at[k, 0])
    take(egb.at[1], s_ex.at[0, 0])
    take(eub.at[1], s_ex.at[1, 0])
    take(edb.at[1], s_ex.at[2, 0])
    take(xa.at[pl.ds(0, 7)], s_xa.at[0])
    take(xc.at[pl.ds(0, 7)], s_xc.at[0])
    take(tb.at[pl.ds(0, 7)], s_ts.at[0])
    take(cb.at[pl.ds(0, 7)], s_cb.at[0])
    take(cd.at[pl.ds(0, 7)], s_cd.at[0])
    take(qr.at[:, pl.ds(0, 7 * BLK)], s_q.at[0])
    take(pr.at[:, pl.ds(0, 7 * BLK)], s_pr.at[0])
    take(zr.at[pl.ds(0, 63)], s_y.at[0])
    take(sqr.at[pl.ds(0, 7)], s_sq.at[0])
    take(zr.at[pl.ds(0, 63)], s_z.at[0])


def shards(
    tokens, cache_keys, cache_values, cache_len, norm_gain_first, w_query, w_key, w_value, head_bias,
    w_output, norm_gain_second, group_id, member, group_gate, member_weight, expert_gate_w, expert_up_w,
    expert_down_w, dense_gate_w, dense_up_w, hidden_gain, dense_down_w, branch_logit,
):
    vmem = pl.BlockSpec(memory_space=pltpu.VMEM)
    hbm = pl.BlockSpec(memory_space=pl.ANY)
    smem = pl.BlockSpec(memory_space=pltpu.SMEM)
    V = pltpu.VMEM
    strips = (8, 2, SEQ, D)
    pair_sem = pltpu.SemaphoreType.DMA((2,))
    args = (
        (tokens, vmem),
        (cache_keys, hbm),
        (cache_values, hbm),
        (cache_len, smem),
        (norm_gain_first.reshape(1, D), vmem),
        (w_query.T, vmem),
        (w_key, hbm),
        (w_value, hbm),
        (head_bias.reshape(1, HEADS), vmem),
        (w_output.T, vmem),
        (norm_gain_second.reshape(1, D), vmem),
        (group_id.reshape(1, SEQ), vmem),
        (member.T, vmem),
        (group_gate.reshape(1, SEQ), vmem),
        (member_weight.T, vmem),
        (expert_gate_w, hbm),
        (expert_up_w, hbm),
        (expert_down_w, hbm),
        (dense_gate_w.T, vmem),
        (dense_up_w.T, vmem),
        (hidden_gain.reshape(1, D), vmem),
        (dense_down_w.T, vmem),
        (branch_logit.reshape(1, D), vmem),
    )
    scratch = [
        V((SEQ, CACHE, 128), BF),
        V((SEQ, CACHE, 128), BF),
        V((2, D, 512), BF),
        V((2, D, 512), BF),
        V((2, 512, D), BF),
        V((D, 128), BF),
        V((D, 128), BF),
        V(strips, BF),
        V(strips, BF),
        V(strips, BF),
        V(strips, BF),
        V((64, 2, SEQ, BLK), BF),
        V((8, SEQ, D), BF),
        V((8, SEQ, D), BF),
        V((8, SEQ, D), BF),
        V((8, SEQ, BLK), BF),
        V((SEQ, D), BF),
        V((8, SEQ, BLK), BF),
        V((8, SEQ, BLK), BF),
        V((SEQ, 128), F32),
        V((8, SEQ, 128), F32),
        V((8, SEQ, 128), F32),
        V((8, SEQ, 128), F32),
        V((512, 512), BF),
        V((512, 512), BF),
        V((512, 128), BF),
        V((SEQ, HEADS, 128), BF),
        V((SEQ, HEADS, 128), BF),
        V((8, SEQ, BLK), BF),
        V((SEQ, D), BF),
        V((8, SEQ, BLK), BF),
        V((8, 128), F32),
        V((8, 8, 128), F32),
        V((8, 8, SEQ, BLK), BF),
        V((8, 8, SEQ, BLK), BF),
        V((64, SEQ, BLK), BF),
        V((128, 1024), BF),
        pltpu.SemaphoreType.DMA((8,)),
        pair_sem,
        pair_sem,
        pair_sem,
        pair_sem,
        pair_sem,
        pltpu.SemaphoreType.DMA((5, 2)),
        pltpu.SemaphoreType.DMA((3, 2)),
    ] + [pair_sem] * 10
    return pl.pallas_call(
        kernel,
        out_shape=(
            jax.ShapeDtypeStruct((SEQ, D), BF),
            jax.ShapeDtypeStruct((SEQ, 128), BF),
            jax.ShapeDtypeStruct((SEQ, 128), BF),
        ),
        in_specs=[spec for _, spec in args],
        out_specs=(vmem, vmem, vmem),
        scratch_shapes=scratch,
        compiler_params=pltpu.CompilerParams(
            collective_id=0, has_side_effects=True, vmem_limit_bytes=62_000_000
        ),
    )(*[a for a, _ in args])


def solution(mesh):
    in_specs = (
        P("ep", None),
        P("ep", None, None),
        P("ep", None, None),
        P("ep"),
        P(),
        P(None, "ep"),
        P(),
        P(),
        P(),
        P(None, "ep"),
        P(),
        P("ep"),
        P("ep", None),
        P("ep"),
        P("ep", None),
        P("ep", None, None),
        P("ep", None, None),
        P("ep", None, None),
        P(None, "ep"),
        P(None, "ep"),
        P(),
        P(None, "ep"),
        P(),
    )
    out_specs = (P("ep", None), P("ep", None), P("ep", None))
    return jax.shard_map(shards, mesh=mesh, in_specs=in_specs, out_specs=out_specs, check_vma=False)
```

time: 318 us -> 238 us (0.75)
  Pallas kernels: 0 us -> 233 us
  waiting for transfers between devices: 156 us -> 0 us
  matrix products: 57.2 us -> 0 us
  local copies, waits for them, and re-layouts: 49.4 us -> 4.02 us
  starting transfers between devices: 23.6 us -> 0 us
  other arithmetic: 15.1 us -> 0 us
  between operations: 14.2 us -> 0.65 us
    pallas_call x0 -> x1, Pallas kernels: none -> 233 us  [shards(): pl.pallas_call(kernel, out_shape=(jax.ShapeDtypeStruct((SEQ, D), BF), jax...]
    all_gather x4 -> x0, waiting for transfers between devices: 115 us -> none  [the longest x1 60.6 us: shards(): lax.all_gather(w_query, 'ep', axis=1, tiled=True)]
    dot_general x18 -> x0, matrix products: 57.2 us -> none  [the longest x1 6.3 us: shards(): jnp.dot(dense_normed, lax.all_gather(dense_down_w, 'ep', axis=1, tiled=Tr...]
    all_to_all x4 -> x0, waiting for transfers between devices: 39.2 us -> none  [the longest x1 17.5 us: shards(): lax.all_to_all(served, 'ep', split_axis=0, concat_axis=0, tiled=True)]
    unnamed x47 -> x3, local copies, waits for them, and re-layouts: 29.6 us -> 4.02 us
    all_to_all x4 -> x0, starting transfers between devices: 23.2 us -> none  [the longest x2 12.6 us: moved(): lax.all_to_all(group, axis, split_axis=split_dim, concat_axis=concat_dim,...]
    slice x2 -> x0, other arithmetic: 10.1 us -> none  [grouped_exchange(): lax.slice_in_dim(a, low, high, axis=item_dim)]
    reshape x7 -> x0, local copies, waits for them, and re-layouts: 7.55 us -> none  [the longest x1 2.71 us: later_sum(): return (within + carried[..., None]).reshape(lead + (span_len,))]
  transfers between devices with their start and end apart: 8 -> 0, of which waited for: 7 -> 0; matrix products, arithmetic and copies ran while one was open for 34% -> 0% of each run, Pallas kernels for 0% -> 0%
where the time goes in v1:
time: 238 us; the launch traced here: 237 us
  Pallas kernels  233 us (98%)
  local copies, waits for them, and re-layouts  4.02 us (2%)
    pallas_call x1, Pallas kernels, shards(): pl.pallas_call(kernel, out_shape=(jax.ShapeDtypeStruct((SEQ, D), BF), jax...  233 us

profile of v1, /device:TPU:0, one launch (start us, length us, event | category | flops | bytes accessed | tf_op | source)
XLA Modules:
  0.0 237.4 jit_solution(992928806766327278)
XLA Ops:
  0.6 232.7 %shard_map.238 = (bf16[16,2048]{1,0:T(8,128)(2,1)}, bf16[16,128]{1,0:T(8,128)(2,1)}, bf16[16,128]{1,0:T(8,128)(2,1)}) custom-call(bf16[16,2048]{1,0:T(8,128)(2,1)} %tok.1, bf16[16,1024,128]{2,1,0:T(8,128)(2,1)} %ck.1, bf16[16,1024,128]{2,1,0:T(8,128)(2,1)} %cv.1, s32[16]{0:T(128)} %clen.1, f32[1,2048]{1,0:T(1,128)} %bitcast.19, bf16[16,2048]{1,0:T(8,128)(2,1)} %bitcast.14, ...), custom_call_target="tpu_custom_call" | custom-call | tf_op jit(solution)/shard_map/pallas_call | solution.py:480
  233.4 1.5 copy.29
  234.8 1.3 copy.30
  236.1 1.3 copy.31

commit v2 on v1

--- a/solution.py
+++ b/solution.py
@@ -57,6 +57,42 @@
     pltpu.make_async_copy(ref, ref, sem).wait()
 
 
+def chip_of(g, p):
+    return g * 8 + (p // 4 + g) % 2 * 4 + p % 4
+
+
+def gather_lanes(tiles, pieces):
+    quarter = iota(tiles[0].shape, 1) // 32
+    made = None
+    for at, (tile, piece) in enumerate(pieces):
+        shift = (at - piece) * 32 % 128
+        v = pltpu.roll(tiles[tile], shift, 1) if shift else tiles[tile]
+        made = v if made is None else jnp.where(quarter == at, v, made)
+    return made
+
+
+def tiles_of(v):
+    return [v[:, t * 128 : (t + 1) * 128] for t in range(D // 128)]
+
+
+def to_block_order(tiles):
+    made = []
+    for t in range(16):
+        p, half = t // 2, t % 2
+        chips = [chip_of(half * 4 + k, p) for k in range(4)]
+        made.append(gather_lanes(tiles, [(c // 4, c % 4) for c in chips]))
+    return made
+
+
+def from_block_order(tiles):
+    made = []
+    for v in range(16):
+        g, yl = v // 2, v % 2
+        places = [(yl + g) % 2 * 4 + x for x in range(4)]
+        made.append(gather_lanes(tiles, [(p * 2 + g // 4, g % 4) for p in places]))
+    return made
+
+
 def lanes(k):
     return pl.ds(pl.multiple_of(k * BLK, BLK), BLK)
 
@@ -67,14 +103,14 @@
     kb, vb, egb, eub, edb, wkb, wvb,
     wqb, wob, wgb, wub, wdb,
     xa, xc, xd, qs, qr, ts, tb, cs0, cb, cs, cd, pq, po, qstack, qb, ob, ps, pr, ys,
-    sq, sqr, zb, zs, zr, hbuf,
+    sq, sqr, zb, zs, zr, hbuf, g2b, hgb, wgp, wup, wdp,
     lsem, s_wq, s_wo, s_wg, s_wu, s_wd, s_pair, s_ex, s_xa, s_xc, s_ts, s_cb, s_cd, s_q, s_pr, s_y, s_sq, s_z,
 ):
     me = lax.axis_index("ep")
     chip = me // 2
     core = me % 2
     group = me // 16
-    place = chip % 8
+    place = (chip % 8 // 4 + group) % 2 * 4 + chip % 4
     pair = chip * 2 + (1 - core)
 
     local = [
@@ -82,10 +118,15 @@
         pltpu.make_async_copy(cv, vb, lsem.at[1]),
         pltpu.make_async_copy(wk, wkb, lsem.at[2]),
         pltpu.make_async_copy(wv, wvb, lsem.at[3]),
-        pltpu.make_async_copy(eg.at[0], egb.at[0], lsem.at[4]),
-        pltpu.make_async_copy(eu.at[0], eub.at[0], lsem.at[5]),
-        pltpu.make_async_copy(ed.at[0], edb.at[0], lsem.at[6]),
+        pltpu.make_async_copy(ed.at[0], edb.at[0], lsem.at[4]),
     ]
+
+    def load_experts(k, carry):
+        src = pl.ds(pl.multiple_of(chip_of(k % 8, k // 8) * 32, 32), 32)
+        dst = pl.ds(pl.multiple_of(k * 32, 32), 32)
+        pltpu.make_async_copy(eg.at[0, src], egb.at[0, dst], lsem.at[5]).start()
+        pltpu.make_async_copy(eu.at[0, src], eub.at[0, dst], lsem.at[6]).start()
+        return carry
 
     barrier = pltpu.get_barrier_semaphore()
 
@@ -98,6 +139,7 @@
     lax.fori_loop(1, 64, greet, 0)
     for c in local:
         c.start()
+    lax.fori_loop(0, 64, load_experts, 0)
 
     x = tok[...].astype(F32)
     normed = (x * lax.rsqrt(jnp.mean(x * x, axis=-1, keepdims=True) + EPS) * g1[...]).astype(BF)
@@ -112,44 +154,26 @@
     spot_col = jnp.sum(jnp.where(eye16, jnp.broadcast_to(spot, (SEQ, SEQ)), 0), axis=1, keepdims=True)
     back = one_hot(iota((SEQ, SEQ), 1) == spot_col).astype(BF)
     order_bf = order.astype(BF)
-    sorted_tok = dot(order_bf, tok[...]).astype(BF)
-    for k in range(8):
-        ts[k] = sorted_tok[:, k * BLK : (k + 1) * BLK]
     share = jnp.zeros((128, SEQ), F32)
     for k in range(6):
         share = share + jnp.where(iota((128, SEQ), 0) == mem[k : k + 1, :], mw[k : k + 1, :], 0.0)
     share = share * gg[...]
     shared = lax.dot_general(order, share, NT, precision=HI, preferred_element_type=F32)
     cs0[...] = shared
-    tb[place] = ts[place]
     cb[place] = shared
 
     pl.semaphore_wait(barrier, 64)
 
     def spread_strip(strip, buf, sems):
-        slot = buf.at[place, core]
+        slot = buf.at[group, core]
 
         def send(k, carry):
             g = (group + k) % 8
-            remote(strip, slot, sems, (g * 8 + group) * 2 + core).start()
+            remote(strip, slot, sems, chip_of(g, place) * 2 + core).start()
             return carry
 
-        @pl.when(place == group)
-        def _():
-            pltpu.make_async_copy(strip, slot, sems.at[1]).start()
-
-        @pl.when(place != group)
-        def _():
-            send(0, 0)
-
+        pltpu.make_async_copy(strip, slot, sems.at[1]).start()
         lax.fori_loop(1, 8, send, 0)
-
-    def strip_sent(strip, buf, sems):
-        take(buf.at[pl.ds(0, 7), core], sems.at[0])
-
-        @pl.when(place != group)
-        def _():
-            take(buf.at[0, core], sems.at[0])
 
     def pass_on(buf, sems, k):
         take(buf.at[:, core], sems.at[1])
@@ -158,7 +182,7 @@
     def in_group(src_of, dst, sems):
         def send(k, carry):
             p = (place + k) % 8
-            remote(src_of(p), dst, sems, (group * 8 + p) * 2 + core).start()
+            remote(src_of(p), dst, sems, chip_of(group, p) * 2 + core).start()
             return carry
 
         lax.fori_loop(1, 8, send, 0)
@@ -173,9 +197,16 @@
 
     spread_strip(wq, wqb, s_wq)
     in_group(lambda p: xa.at[place], xa.at[place], s_xa)
+    in_group(lambda p: cs0, cb.at[place], s_cb)
+
+    moved = to_block_order(tiles_of(dot(order_bf, tok[...])))
+    for k in range(8):
+        ts[k] = jnp.concatenate(moved[2 * k : 2 * k + 2], axis=1).astype(BF)
+    tb[place] = ts[place]
     in_group(lambda p: ts.at[p], tb.at[place], s_ts)
-    in_group(lambda p: cs0, cb.at[place], s_cb)
-
+    for src, dst in ((g2, g2b), (hg, hgb), (wg, wgp), (wu, wup), (wd, wdp)):
+        for k, tile in enumerate(to_block_order(tiles_of(src[...].astype(F32)))):
+            dst[:, k * 128 : (k + 1) * 128] = tile.astype(dst.dtype)
     local[2].wait()
     local[3].wait()
     nk[...] = dot(normed, wkb[...]).astype(BF)
@@ -200,9 +231,9 @@
     in_group(lambda p: qs.at[p], qr.at[:, lanes(place)], s_q)
 
     spread_strip(wo, wob, s_wo)
-    remote(eg.at[0], egb.at[1], s_ex.at[0], pair).start()
-    remote(eu.at[0], eub.at[1], s_ex.at[1], pair).start()
-    remote(ed.at[0], edb.at[1], s_ex.at[2], pair).start()
+    for k, buf in enumerate((edb, egb, eub)):
+        take(buf.at[0], lsem.at[4 + k])
+        remote(buf.at[0], buf.at[1], s_ex.at[k], pair).start()
 
     take(tb.at[pl.ds(0, 7)], s_ts.at[1])
     take(cb.at[pl.ds(0, 7)], s_cb.at[1])
@@ -212,15 +243,14 @@
 
     def send_comb(k, carry):
         g = (group + k) % 8
-        remote(cs.at[g], cd.at[group], s_cd, (g * 8 + place) * 2 + core).start()
+        remote(cs.at[g], cd.at[group], s_cd, chip_of(g, place) * 2 + core).start()
         return carry
 
     lax.fori_loop(1, 8, send_comb, 0)
 
     take(qr.at[:, pl.ds(0, 7 * BLK)], s_q.at[1])
     left = iota((SEQ, 128), 1) < HEAD_DIM
-    for t in range(16):
-        v = qr[:, t * 128 : (t + 1) * 128].astype(F32) * HEAD_DIM**-0.5
+    for t, v in enumerate(from_block_order(tiles_of(qr[...].astype(F32) * HEAD_DIM**-0.5))):
         w = pltpu.roll(v, HEAD_DIM, 1)
         first, second = (v, w) if t < 8 else (w, v)
         keep = left if t < 8 else jnp.logical_not(left)
@@ -229,8 +259,8 @@
     qb[...] = dot(pq[...], qstack[...]).astype(BF).reshape(SEQ, HEADS, 128)
     local[0].wait()
     local[1].wait()
-    spread_strip(wg, wgb, s_wg)
-    spread_strip(wu, wub, s_wu)
+    spread_strip(wgp, wgb, s_wg)
+    spread_strip(wup, wub, s_wu)
 
     def attend(b, carry):
         s = dot_nt(qb[b], kb[b]) + bias
@@ -265,15 +295,15 @@
         xc[place, :, t * 128 : (t + 1) * 128] = dot(order_bf, joined.astype(BF)).astype(BF)
     in_group(lambda p: xc.at[place], xc.at[place], s_xc)
 
-    over_plane(lambda o: wd.at[:, lanes(o % 8)], lambda o: wdb.at[chip, core], s_wd)
-    own_wd = pltpu.make_async_copy(wd.at[:, lanes(place)], wdb.at[chip, core], lsem.at[7])
+    over_plane(lambda o: wdp.at[:, lanes((o % 8 // 4 + o // 8) % 2 * 4 + o % 4)], lambda o: wdb.at[chip, core], s_wd)
+    own_wd = pltpu.make_async_copy(wdp.at[:, lanes(place)], wdb.at[chip, core], lsem.at[7])
     own_wd.start()
 
     take(wob.at[:, core], s_pair.at[1, 1])
     take(xc.at[pl.ds(0, 7)], s_xc.at[1])
     proj = dot_nt(xc[...].reshape(128, D), wob[...].reshape(BLK, D)).astype(BF)
     stream = tb[...].reshape(128, BLK).astype(F32) + proj.astype(F32)
-    y = (stream * g2[:, lanes(place)]).astype(BF)
+    y = (stream * g2b[:, lanes(place)]).astype(BF)
     ys[...] = dot(regroup.astype(BF), y).astype(BF).reshape(8, SEQ, BLK)
     xd[group, :, lanes(place)] = ys[group]
     over_plane(lambda o: ys.at[o // 8], lambda o: xd.at[group, :, lanes(place)], s_y)
@@ -289,14 +319,14 @@
     take(cd.at[pl.ds(0, 7)], s_cd.at[1])
     lane = iota((128, 128), 1)
     comb = cd[...].reshape(128, 128)
-    member0 = place * 2 + core
-    member1 = place * 2 + 1 - core
+    member0 = chip % 8 * 2 + core
+    member1 = chip % 8 * 2 + 1 - core
     comb0 = jnp.sum(jnp.where(lane == member0, comb, 0.0), axis=1, keepdims=True)
     comb1 = jnp.sum(jnp.where(lane == member1, comb, 0.0), axis=1, keepdims=True)
 
     take(zr.at[pl.ds(0, 63)], s_y.at[1])
     rows_in = xd[...].reshape(128, D)
-    plain = rows_in.astype(F32) * (1.0 / g2[...])
+    plain = rows_in.astype(F32) * (1.0 / g2b[...])
     scale = lax.rsqrt(jnp.mean(plain * plain, axis=1, keepdims=True) + EPS)
     take(wgb.at[:, core], s_pair.at[2, 1])
     take(wub.at[:, core], s_pair.at[3, 1])
@@ -310,13 +340,10 @@
     in_group(lambda p: sq, sqr.at[place], s_sq)
 
     for e, comb_e in ((0, comb0), (1, comb1)):
-        if e == 0:
-            for k in (4, 5, 6):
-                local[k].wait()
-        else:
-            take(egb.at[1], s_ex.at[0, 1])
-            take(eub.at[1], s_ex.at[1, 1])
-            take(edb.at[1], s_ex.at[2, 1])
+        if e == 1:
+            take(edb.at[1], s_ex.at[0, 1])
+            take(egb.at[1], s_ex.at[1, 1])
+            take(eub.at[1], s_ex.at[2, 1])
         gate_e = dot(rows_in, egb[e]) * scale
         upper_e = dot(rows_in, eub[e]) * scale
         hbuf[:, e * 512 : (e + 1) * 512] = (gate_e * jax.nn.sigmoid(gate_e) * upper_e * comb_e).astype(BF)
@@ -325,7 +352,7 @@
     total = jnp.sum(sqr[...], axis=0)[0:1, :]
     total_col = jnp.sum(jnp.where(eye, jnp.broadcast_to(total, (128, 128)), 0.0), axis=1, keepdims=True)
     dense_scale = lax.rsqrt(total_col * (1.0 / D) + EPS)
-    dense = (hidden * dense_scale * hg[:, lanes(place)]).astype(BF)
+    dense = (hidden * dense_scale * hgb[:, lanes(place)]).astype(BF)
     take(wdb.at[:, core], s_pair.at[4, 1])
 
     def produce(k, carry):
@@ -343,7 +370,7 @@
 
         def send(j, carry):
             p = (place + j) % 8
-            remote(zs.at[g, p], zr.at[chip], s_z, (g * 8 + p) * 2 + core).start()
+            remote(zs.at[g, p], zr.at[chip], s_z, chip_of(g, p) * 2 + core).start()
             return carry
 
         @pl.when(g == group)
@@ -363,25 +390,26 @@
     unfold = dot(spots, one_hot(iota((SEQ, 128), 1) // 8 == iota((SEQ, 128), 0)))
     unfold = jnp.where(r // 16 == c % 8, unfold, 0.0).astype(BF)
     take(pr.at[:, pl.ds(0, 7 * BLK)], s_pr.at[1])
-    second = tok[...].astype(F32) + dot(back, pr[...])
+    second = from_block_order(tiles_of(dot(back, pr[...])))
     take(zr.at[pl.ds(0, 63)], s_z.at[1])
     sums = jnp.sum(zr[...].reshape(8, 8, SEQ, BLK).astype(F32), axis=1).reshape(128, BLK)
     high, low = split2(sums)
     branch = dot(unfold, high) + dot(unfold, low)
     for k in range(8):
         s = slice(k * BLK, (k + 1) * BLK)
-        out[:, s] = (second[:, s] + branch[k * 16 : k * 16 + 16]).astype(BF)
-
-    strip_sent(wq, wqb, s_wq)
-    strip_sent(wo, wob, s_wo)
-    strip_sent(wg, wgb, s_wg)
-    strip_sent(wu, wub, s_wu)
+        own = tok[:, s].astype(F32) + jnp.concatenate(second[2 * k : 2 * k + 2], axis=1)
+        out[:, s] = (own + branch[k * 16 : k * 16 + 16]).astype(BF)
+
+    take(wqb.at[pl.ds(0, 7), core], s_wq.at[0])
+    take(wob.at[pl.ds(0, 7), core], s_wo.at[0])
+    take(wgb.at[pl.ds(0, 7), core], s_wg.at[0])
+    take(wub.at[pl.ds(0, 7), core], s_wu.at[0])
     take(wdb.at[pl.ds(0, 63), core], s_wd.at[0])
     for k, buf in enumerate((wqb, wob, wgb, wub, wdb)):
         take(buf.at[:, core], s_pair.at[k, 0])
-    take(egb.at[1], s_ex.at[0, 0])
-    take(eub.at[1], s_ex.at[1, 0])
-    take(edb.at[1], s_ex.at[2, 0])
+    take(edb.at[1], s_ex.at[0, 0])
+    take(egb.at[1], s_ex.at[1, 0])
+    take(eub.at[1], s_ex.at[2, 0])
     take(xa.at[pl.ds(0, 7)], s_xa.at[0])
     take(xc.at[pl.ds(0, 7)], s_xc.at[0])
     take(tb.at[pl.ds(0, 7)], s_ts.at[0])
@@ -468,6 +496,11 @@
         V((8, 8, SEQ, BLK), BF),
         V((64, SEQ, BLK), BF),
         V((128, 1024), BF),
+        V((1, D), F32),
+        V((1, D), F32),
+        V((SEQ, D), BF),
+        V((SEQ, D), BF),
+        V((SEQ, D), BF),
         pltpu.SemaphoreType.DMA((8,)),
         pair_sem,
         pair_sem,

time: 238 us -> 80.1 us (0.34)
  Pallas kernels: 233 us -> 75.1 us
    pallas_call x1, Pallas kernels: 233 us -> 75.1 us  [shards(): pl.pallas_call(kernel, out_shape=(jax.ShapeDtypeStruct((SEQ, D), BF), jax...]
where the time goes in v2:
time: 80.1 us; the launch traced here: 79.8 us
  Pallas kernels  75.1 us (94%)
  local copies, waits for them, and re-layouts  4.02 us (5%)
    pallas_call x1, Pallas kernels, shards(): pl.pallas_call(kernel, out_shape=(jax.ShapeDtypeStruct((SEQ, D), BF), jax...  75.1 us
    unnamed x3, local copies, waits for them, and re-layouts  4.02 us

profile of v2, /device:TPU:0, one launch (start us, length us, event | category | flops | bytes accessed | tf_op | source)
XLA Modules:
  0.0 79.8 jit_solution(3799506131739492357)
XLA Ops:
  0.6 75.1 %shard_map.238 = (bf16[16,2048]{1,0:T(8,128)(2,1)}, bf16[16,128]{1,0:T(8,128)(2,1)}, bf16[16,128]{1,0:T(8,128)(2,1)}) custom-call(bf16[16,2048]{1,0:T(8,128)(2,1)} %tok.1, bf16[16,1024,128]{2,1,0:T(8,128)(2,1)} %ck.1, bf16[16,1024,128]{2,1,0:T(8,128)(2,1)} %cv.1, s32[16]{0:T(128)} %clen.1, f32[1,2048]{1,0:T(1,128)} %bitcast.19, bf16[16,2048]{1,0:T(8,128)(2,1)} %bitcast.14, ...), custom_call_target="tpu_custom_call" | custom-call | tf_op jit(solution)/shard_map/pallas_call | solution.py:513
  75.8 1.5 %copy.29 = bf16[16,2048]{1,0:T(8,128)(2,1)} copy(bf16[16,2048]{1,0:T(8,128)(2,1)} %get-tuple-element.6) | data formatting | bytes 131072
  77.3 1.3 %copy.30 = bf16[16,128]{1,0:T(8,128)(2,1)} copy(bf16[16,128]{1,0:T(8,128)(2,1)} %get-tuple-element.7) | data formatting | bytes 8192
  78.5 1.3 %copy.31 = bf16[16,128]{1,0:T(8,128)(2,1)} copy(bf16[16,128]{1,0:T(8,128)(2,1)} %get-tuple-element.8) | data formatting | bytes 8192

commit v3 on v2

--- a/solution.py
+++ b/solution.py
@@ -103,8 +103,8 @@
     kb, vb, egb, eub, edb, wkb, wvb,
     wqb, wob, wgb, wub, wdb,
     xa, xc, xd, qs, qr, ts, tb, cs0, cb, cs, cd, pq, po, qstack, qb, ob, ps, pr, ys,
-    sq, sqr, zb, zs, zr, hbuf, g2b, hgb, wgp, wup, wdp,
-    lsem, s_wq, s_wo, s_wg, s_wu, s_wd, s_pair, s_ex, s_xa, s_xc, s_ts, s_cb, s_cd, s_q, s_pr, s_y, s_sq, s_z,
+    sq, sqr, zb, zs, zr, hbuf, zf, sc, wt, g2b, hgb, wgp, wup, wdp,
+    lsem, s_wq, s_wo, s_wg, s_wu, s_wd, s_pair, s_ex, s_xa, s_xc, s_ts, s_cb, s_cd, s_q, s_pr, s_y, s_sq, s_z, s_wq2, s_xc2,
 ):
     me = lax.axis_index("ep")
     chip = me // 2
@@ -151,14 +151,11 @@
     spot = gids * 2 + rank
     order = one_hot(iota((SEQ, SEQ), 0) == spot)
     eye16 = iota((SEQ, SEQ), 0) == iota((SEQ, SEQ), 1)
-    spot_col = jnp.sum(jnp.where(eye16, jnp.broadcast_to(spot, (SEQ, SEQ)), 0), axis=1, keepdims=True)
-    back = one_hot(iota((SEQ, SEQ), 1) == spot_col).astype(BF)
-    order_bf = order.astype(BF)
     share = jnp.zeros((128, SEQ), F32)
     for k in range(6):
         share = share + jnp.where(iota((128, SEQ), 0) == mem[k : k + 1, :], mw[k : k + 1, :], 0.0)
-    share = share * gg[...]
-    shared = lax.dot_general(order, share, NT, precision=HI, preferred_element_type=F32)
+    share = share * gg[...] + jnp.where(iota((128, SEQ), 0) == SEQ, spot.astype(F32), 0.0)
+    shared = lax.dot_general(one_hot(eye16), share, NT, precision=HI, preferred_element_type=F32)
     cs0[...] = shared
     cb[place] = shared
 
@@ -193,13 +190,16 @@
             remote(src_of(other), dst_of(other), sems, other * 2 + core).start()
             return carry
 
-        lax.fori_loop(1, 64, send, 0)
-
-    spread_strip(wq, wqb, s_wq)
+        lax.fori_loop(1, 64, send, 0, unroll=7)
+
+    near, far = pl.ds(0, D // 2), pl.ds(D // 2, D // 2)
+    spread_strip(wq.at[:, near], wqb.at[:, :, :, near], s_wq)
+    spread_strip(wq.at[:, far], wqb.at[:, :, :, far], s_wq2)
     in_group(lambda p: xa.at[place], xa.at[place], s_xa)
     in_group(lambda p: cs0, cb.at[place], s_cb)
-
-    moved = to_block_order(tiles_of(dot(order_bf, tok[...])))
+    spread_strip(wo, wob, s_wo)
+
+    moved = to_block_order(tiles_of(tok[...].astype(F32)))
     for k in range(8):
         ts[k] = jnp.concatenate(moved[2 * k : 2 * k + 2], axis=1).astype(BF)
     tb[place] = ts[place]
@@ -207,37 +207,47 @@
     for src, dst in ((g2, g2b), (hg, hgb), (wg, wgp), (wu, wup), (wd, wdp)):
         for k, tile in enumerate(to_block_order(tiles_of(src[...].astype(F32)))):
             dst[:, k * 128 : (k + 1) * 128] = tile.astype(dst.dtype)
+    spread_strip(wgp, wgb, s_wg)
+    spread_strip(wup, wub, s_wu)
     local[2].wait()
     local[3].wait()
     nk[...] = dot(normed, wkb[...]).astype(BF)
     nv[...] = dot(normed, wvb[...]).astype(BF)
     rows, cols = iota((512, 512), 0), iota((512, 512), 1)
     pq[...] = one_hot(cols == rows % 32 * 16 + rows // 32).astype(BF)
-    po[...] = one_hot(cols == rows % 16 * 32 + rows // 16).astype(BF)
+    rows, cols = iota((256, 256), 0), iota((256, 256), 1)
+    po[...] = one_hot(cols == rows % 8 * 32 + rows // 8).astype(BF)
     r, c = iota((128, 128), 0), iota((128, 128), 1)
-    regroup = one_hot(c == r % 16 // 2 * 16 + r // 16 * 2 + r % 2)
     fold = one_hot(c == r % 8 * 16 + r // 16 * 2 + r % 16 // 8).astype(BF)
     eye = r == c
     eye32 = iota((32, 32), 0) == iota((32, 32), 1)
     bias = jnp.sum(jnp.where(eye32, jnp.broadcast_to(hb[...], (32, 32)), 0.0), axis=1, keepdims=True)
     tri = one_hot(iota((BLK, BLK), 0) >= iota((BLK, BLK), 1)).astype(BF)
 
-    pass_on(wqb, s_wq, 0)
+    pass_on(wqb.at[:, :, :, near], s_wq, 0)
+    pass_on(wqb.at[:, :, :, far], s_wq2, 5)
     take(xa.at[pl.ds(0, 7)], s_xa.at[1])
-    take(wqb.at[:, core], s_pair.at[0, 1])
-    q = dot_nt(xa[...].reshape(128, D), wqb[...].reshape(BLK, D)).astype(BF)
+    take(wqb.at[:, core, :, near], s_pair.at[0, 1])
+    q = dot_nt(xa[:, :, : D // 2].reshape(128, D // 2), wqb[:, :, :, : D // 2].reshape(BLK, D // 2))
+    take(wqb.at[:, core, :, far], s_pair.at[5, 1])
+    q = q + dot_nt(xa[:, :, D // 2 :].reshape(128, D // 2), wqb[:, :, :, D // 2 :].reshape(BLK, D // 2))
+    q = q.astype(BF)
     qs[...] = q.reshape(8, SEQ, BLK)
     qr[:, lanes(place)] = qs[place]
     in_group(lambda p: qs.at[p], qr.at[:, lanes(place)], s_q)
 
-    spread_strip(wo, wob, s_wo)
     for k, buf in enumerate((edb, egb, eub)):
         take(buf.at[0], lsem.at[4 + k])
         remote(buf.at[0], buf.at[1], s_ex.at[k], pair).start()
 
     take(tb.at[pl.ds(0, 7)], s_ts.at[1])
     take(cb.at[pl.ds(0, 7)], s_cb.at[1])
-    combs = jnp.dot(regroup, cb[...].reshape(128, 128), precision=HI, preferred_element_type=F32)
+    sent = cb[...].reshape(128, 128)
+    spot_row = jnp.sum(jnp.where(eye, jnp.broadcast_to(sent[:, SEQ : SEQ + 1], (128, 128)), 0.0), axis=0, keepdims=True)
+    wanted = (r // 16 * 2 + r % 2).astype(F32)
+    regroup = jnp.where(c // 16 == r % 16 // 2, one_hot(wanted == jnp.broadcast_to(spot_row, (128, 128))), 0.0)
+    regroup_bf = regroup.astype(BF)
+    combs = jnp.dot(regroup, sent, precision=HI, preferred_element_type=F32)
     cs[...] = combs.reshape(8, SEQ, 128)
     cd[group] = cs[group]
 
@@ -247,6 +257,10 @@
         return carry
 
     lax.fori_loop(1, 8, send_comb, 0)
+
+    over_plane(lambda o: wdp.at[:, lanes((o % 8 // 4 + o // 8) % 2 * 4 + o % 4)], lambda o: wdb.at[chip, core], s_wd)
+    own_wd = pltpu.make_async_copy(wdp.at[:, lanes(place)], wdb.at[chip, core], lsem.at[7])
+    own_wd.start()
 
     take(qr.at[:, pl.ds(0, 7 * BLK)], s_q.at[1])
     left = iota((SEQ, 128), 1) < HEAD_DIM
@@ -259,52 +273,70 @@
     qb[...] = dot(pq[...], qstack[...]).astype(BF).reshape(SEQ, HEADS, 128)
     local[0].wait()
     local[1].wait()
-    spread_strip(wgp, wgb, s_wg)
-    spread_strip(wup, wub, s_wu)
-
-    def attend(b, carry):
-        s = dot_nt(qb[b], kb[b]) + bias
-        live = iota((HEADS, CACHE), 1) < clen[b]
-        rest = jnp.where(live, -(jnp.maximum(s, 0.0) + jnp.log(1.0 + jnp.exp(-jnp.abs(s)))), 0.0)
-        high, low = split2(rest)
-        parts = [v[:, n * BLK : (n + 1) * BLK] for v in (high, low) for n in range(4)]
+
+    def score(t):
+        for k in range(2):
+            sc[t % 2, k] = dot_nt(qb[2 * t + k], kb[2 * t + k]) + bias
+
+    def weigh(t):
+        parts = []
+        for k in range(2):
+            length = clen[2 * t + k]
+            for n in range(4):
+                v = sc[t % 2, k, :, n * BLK : (n + 1) * BLK]
+                live = iota((HEADS, BLK), 1) < length - n * BLK
+                rest = jnp.where(live, -(jnp.maximum(v, 0.0) + jnp.log(1.0 + jnp.exp(-jnp.abs(v)))), 0.0)
+                parts.extend(split2(rest))
         sums = dot(jnp.concatenate(parts, axis=0), tri)
-        run = jnp.zeros((HEADS, 1), F32)
-        later = []
-        for n in (3, 2, 1, 0):
-            within = sums[n * 32 : n * 32 + 32] + sums[128 + n * 32 : 160 + n * 32]
-            later.append(within + run)
-            run = run + within[:, 0:1]
-        later = jnp.concatenate(later[::-1], axis=1)
-        weights = jnp.where(live, jnp.exp(s + later), 0.0).astype(BF)
-        ob[b] = dot(weights, vb[b]).astype(BF)
-        return carry
-
-    lax.fori_loop(0, 8, attend, 0)
-    pass_on(wob, s_wo, 1)
-    lax.fori_loop(8, 16, attend, 0)
-
-    heads = dot(po[...], ob[...].reshape(512, 128))
-    for t in range(16):
-        a = heads[32 * t : 32 * t + 16, :]
-        b = heads[32 * t + 16 : 32 * t + 32, :]
+        for k in range(2):
+            length = clen[2 * t + k]
+            run = jnp.zeros((HEADS, 1), F32)
+            for n in (3, 2, 1, 0):
+                at = (k * 4 + n) * 64
+                within = sums[at : at + 32] + sums[at + 32 : at + 64]
+                live = iota((HEADS, BLK), 1) < length - n * BLK
+                v = sc[t % 2, k, :, n * BLK : (n + 1) * BLK]
+                wt[t % 2, k, :, n * BLK : (n + 1) * BLK] = jnp.where(live, jnp.exp(v + within + run), 0.0).astype(BF)
+                run = run + within[:, 0:1]
+
+    def mix(t):
+        for k in range(2):
+            ob[2 * t + k] = dot(wt[t % 2, k], vb[2 * t + k]).astype(BF)
+
+    def hand_out(half):
+        rows8 = slice(half * 8, half * 8 + 8)
+        heads = dot(po[...], ob[rows8].reshape(256, 128))
+        left8 = iota((8, 128), 1) < HEAD_DIM
+        for t in range(16):
+            a = heads[16 * t : 16 * t + 8, :]
+            b = heads[16 * t + 8 : 16 * t + 16, :]
+            if t < 8:
+                joined = jnp.where(left8, a, pltpu.roll(b, HEAD_DIM, 1))
+            else:
+                joined = jnp.where(left8, pltpu.roll(a, HEAD_DIM, 1), b)
+            xc[place, rows8, t * 128 : (t + 1) * 128] = joined.astype(BF)
+        part = xc.at[place, pl.ds(half * 8, 8)]
+        in_group(lambda p: part, part, s_xc if half == 0 else s_xc2)
+
+    for t in range(10):
         if t < 8:
-            joined = jnp.where(left, a, pltpu.roll(b, HEAD_DIM, 1))
-        else:
-            joined = jnp.where(left, pltpu.roll(a, HEAD_DIM, 1), b)
-        xc[place, :, t * 128 : (t + 1) * 128] = dot(order_bf, joined.astype(BF)).astype(BF)
-    in_group(lambda p: xc.at[place], xc.at[place], s_xc)
-
-    over_plane(lambda o: wdp.at[:, lanes((o % 8 // 4 + o // 8) % 2 * 4 + o % 4)], lambda o: wdb.at[chip, core], s_wd)
-    own_wd = pltpu.make_async_copy(wdp.at[:, lanes(place)], wdb.at[chip, core], lsem.at[7])
-    own_wd.start()
+            score(t)
+        if 1 <= t < 9:
+            weigh(t - 1)
+        if t >= 2:
+            mix(t - 2)
+        if t == 5:
+            hand_out(0)
+            pass_on(wob, s_wo, 1)
+    hand_out(1)
 
     take(wob.at[:, core], s_pair.at[1, 1])
-    take(xc.at[pl.ds(0, 7)], s_xc.at[1])
+    take(xc.at[pl.ds(0, 7), pl.ds(0, 8)], s_xc.at[1])
+    take(xc.at[pl.ds(0, 7), pl.ds(0, 8)], s_xc2.at[1])
     proj = dot_nt(xc[...].reshape(128, D), wob[...].reshape(BLK, D)).astype(BF)
     stream = tb[...].reshape(128, BLK).astype(F32) + proj.astype(F32)
     y = (stream * g2b[:, lanes(place)]).astype(BF)
-    ys[...] = dot(regroup.astype(BF), y).astype(BF).reshape(8, SEQ, BLK)
+    ys[...] = dot(regroup_bf, y).astype(BF).reshape(8, SEQ, BLK)
     xd[group, :, lanes(place)] = ys[group]
     over_plane(lambda o: ys.at[o // 8], lambda o: xd.at[group, :, lanes(place)], s_y)
     ps[...] = proj.reshape(8, SEQ, BLK)
@@ -348,6 +380,11 @@
         upper_e = dot(rows_in, eub[e]) * scale
         hbuf[:, e * 512 : (e + 1) * 512] = (gate_e * jax.nn.sigmoid(gate_e) * upper_e * comb_e).astype(BF)
 
+    def route(k, carry):
+        zf[:, lanes(k)] = dot(hbuf[...], edb[:, :, lanes(k)].reshape(1024, BLK))
+        return carry
+
+    lax.fori_loop(0, 8, route, 0, unroll=2)
     take(sqr.at[pl.ds(0, 7)], s_sq.at[1])
     total = jnp.sum(sqr[...], axis=0)[0:1, :]
     total_col = jnp.sum(jnp.where(eye, jnp.broadcast_to(total, (128, 128)), 0.0), axis=1, keepdims=True)
@@ -356,13 +393,12 @@
     take(wdb.at[:, core], s_pair.at[4, 1])
 
     def produce(k, carry):
-        routed = dot(hbuf[...], edb[:, :, lanes(k)].reshape(1024, BLK))
         down = dot_nt(dense, wdb[pl.ds(k * 8, 8)].reshape(BLK, BLK))
-        z = routed + jax.nn.sigmoid(bl[:, lanes(k)]) * down
+        z = zf[:, lanes(k)] + jax.nn.sigmoid(bl[:, lanes(k)]) * down
         zb[k] = z.astype(BF).reshape(8, SEQ, BLK)
         return carry
 
-    lax.fori_loop(0, 8, produce, 0)
+    lax.fori_loop(0, 8, produce, 0, unroll=2)
 
     def give(k, carry):
         g = (group + k) % 8
@@ -390,7 +426,7 @@
     unfold = dot(spots, one_hot(iota((SEQ, 128), 1) // 8 == iota((SEQ, 128), 0)))
     unfold = jnp.where(r // 16 == c % 8, unfold, 0.0).astype(BF)
     take(pr.at[:, pl.ds(0, 7 * BLK)], s_pr.at[1])
-    second = from_block_order(tiles_of(dot(back, pr[...])))
+    second = from_block_order(tiles_of(pr[...].astype(F32)))
     take(zr.at[pl.ds(0, 63)], s_z.at[1])
     sums = jnp.sum(zr[...].reshape(8, 8, SEQ, BLK).astype(F32), axis=1).reshape(128, BLK)
     high, low = split2(sums)
@@ -400,18 +436,20 @@
         own = tok[:, s].astype(F32) + jnp.concatenate(second[2 * k : 2 * k + 2], axis=1)
         out[:, s] = (own + branch[k * 16 : k * 16 + 16]).astype(BF)
 
-    take(wqb.at[pl.ds(0, 7), core], s_wq.at[0])
+    take(wqb.at[pl.ds(0, 7), core, :, near], s_wq.at[0])
+    take(wqb.at[pl.ds(0, 7), core, :, far], s_wq2.at[0])
     take(wob.at[pl.ds(0, 7), core], s_wo.at[0])
     take(wgb.at[pl.ds(0, 7), core], s_wg.at[0])
     take(wub.at[pl.ds(0, 7), core], s_wu.at[0])
     take(wdb.at[pl.ds(0, 63), core], s_wd.at[0])
-    for k, buf in enumerate((wqb, wob, wgb, wub, wdb)):
+    for k, buf in enumerate((wqb.at[:, :, :, near], wob, wgb, wub, wdb, wqb.at[:, :, :, far])):
         take(buf.at[:, core], s_pair.at[k, 0])
     take(edb.at[1], s_ex.at[0, 0])
     take(egb.at[1], s_ex.at[1, 0])
     take(eub.at[1], s_ex.at[2, 0])
     take(xa.at[pl.ds(0, 7)], s_xa.at[0])
-    take(xc.at[pl.ds(0, 7)], s_xc.at[0])
+    take(xc.at[pl.ds(0, 7), pl.ds(0, 8)], s_xc.at[0])
+    take(xc.at[pl.ds(0, 7), pl.ds(0, 8)], s_xc2.at[0])
     take(tb.at[pl.ds(0, 7)], s_ts.at[0])
     take(cb.at[pl.ds(0, 7)], s_cb.at[0])
     take(cd.at[pl.ds(0, 7)], s_cd.at[0])
@@ -483,7 +521,7 @@
         V((8, SEQ, 128), F32),
         V((8, SEQ, 128), F32),
         V((512, 512), BF),
-        V((512, 512), BF),
+        V((256, 256), BF),
         V((512, 128), BF),
         V((SEQ, HEADS, 128), BF),
         V((SEQ, HEADS, 128), BF),
@@ -496,6 +534,9 @@
         V((8, 8, SEQ, BLK), BF),
         V((64, SEQ, BLK), BF),
         V((128, 1024), BF),
+        V((128, D), F32),
+        V((2, 2, HEADS, CACHE), F32),
+        V((2, 2, HEADS, CACHE), BF),
         V((1, D), F32),
         V((1, D), F32),
         V((SEQ, D), BF),
@@ -507,9 +548,9 @@
         pair_sem,
         pair_sem,
         pair_sem,
-        pltpu.SemaphoreType.DMA((5, 2)),
+        pltpu.SemaphoreType.DMA((6, 2)),
         pltpu.SemaphoreType.DMA((3, 2)),
-    ] + [pair_sem] * 10
+    ] + [pair_sem] * 12
     return pl.pallas_call(
         kernel,
         out_shape=(

time: 80.1 us -> 69.9 us (0.87)
  Pallas kernels: 75.1 us -> 64.9 us
    pallas_call x1, Pallas kernels: 75.1 us -> 64.9 us  [shards(): pl.pallas_call(kernel, out_shape=(jax.ShapeDtypeStruct((SEQ, D), BF), jax...]
where the time goes in v3:
time: 69.9 us; the launch traced here: 69.6 us
  Pallas kernels  64.9 us (93%)
  local copies, waits for them, and re-layouts  4.02 us (6%)
    pallas_call x1, Pallas kernels, shards(): pl.pallas_call(kernel, out_shape=(jax.ShapeDtypeStruct((SEQ, D), BF), jax...  64.9 us
    unnamed x3, local copies, waits for them, and re-layouts  4.02 us

profile of v3, /device:TPU:0, one launch (start us, length us, event | category | flops | bytes accessed | tf_op | source)
XLA Modules:
  0.0 69.6 jit_solution(1446910249502359011)
XLA Ops:
  0.6 64.9 %shard_map.238 = (bf16[16,2048]{1,0:T(8,128)(2,1)}, bf16[16,128]{1,0:T(8,128)(2,1)}, bf16[16,128]{1,0:T(8,128)(2,1)}) custom-call(bf16[16,2048]{1,0:T(8,128)(2,1)} %tok.1, bf16[16,1024,128]{2,1,0:T(8,128)(2,1)} %ck.1, bf16[16,1024,128]{2,1,0:T(8,128)(2,1)} %cv.1, s32[16]{0:T(128)} %clen.1, f32[1,2048]{1,0:T(1,128)} %bitcast.19, bf16[16,2048]{1,0:T(8,128)(2,1)} %bitcast.14, ...), custom_call_target="tpu_custom_call" | custom-call | tf_op jit(solution)/shard_map/pallas_call | solution.py:554
  65.6 1.5 %copy.29 = bf16[16,2048]{1,0:T(8,128)(2,1)} copy(bf16[16,2048]{1,0:T(8,128)(2,1)} %get-tuple-element.6) | data formatting | bytes 131072
  67.1 1.3 %copy.30 = bf16[16,128]{1,0:T(8,128)(2,1)} copy(bf16[16,128]{1,0:T(8,128)(2,1)} %get-tuple-element.7) | data formatting | bytes 8192
  68.3 1.3 %copy.31 = bf16[16,128]{1,0:T(8,128)(2,1)} copy(bf16[16,128]{1,0:T(8,128)(2,1)} %get-tuple-element.8) | data formatting | bytes 8192

commit v4 on v3

--- a/solution.py
+++ b/solution.py
@@ -98,13 +98,14 @@
 
 
 def kernel(
-    tok, ck, cv, clen, g1, wq, wk, wv, hb, wo, g2, gid, mem, gg, mw, eg, eu, ed, wg, wu, hg, wd, bl,
+    tok_h, ck, cv, clen_h, g1_h, wq_h, wk, wv, hb_h, wo_h, g2_h, gid_h, mem_h, gg_h, mw_h, eg, eu, ed, wg_h, wu_h, hg_h, wd_h, bl_h,
     out, nk, nv,
     kb, vb, egb, eub, edb, wkb, wvb,
     wqb, wob, wgb, wub, wdb,
     xa, xc, xd, qs, qr, ts, tb, cs0, cb, cs, cd, pq, po, qstack, qb, ob, ps, pr, ys,
     sq, sqr, zb, zs, zr, hbuf, zf, sc, wt, g2b, hgb, wgp, wup, wdp,
     lsem, s_wq, s_wo, s_wg, s_wu, s_wd, s_pair, s_ex, s_xa, s_xc, s_ts, s_cb, s_cd, s_q, s_pr, s_y, s_sq, s_z, s_wq2, s_xc2,
+    tok, clen, g1, wq, hb, wo, g2, gid, mem, gg, mw, wg, wu, hg, wd, bl, fsem,
 ):
     me = lax.axis_index("ep")
     chip = me // 2
@@ -113,6 +114,15 @@
     place = (chip % 8 // 4 + group) % 2 * 4 + chip % 4
     pair = chip * 2 + (1 - core)
 
+    fetch = [
+        pltpu.make_async_copy(src, dst, fsem.at[k])
+        for k, (src, dst) in enumerate(
+            (
+                (tok_h, tok), (g1_h, g1), (gid_h, gid), (mem_h, mem), (mw_h, mw), (gg_h, gg), (clen_h, clen), (hb_h, hb),
+                (wq_h, wq), (wo_h, wo), (g2_h, g2), (hg_h, hg), (wg_h, wg), (wu_h, wu), (wd_h, wd), (bl_h, bl),
+            )
+        )
+    ]
     local = [
         pltpu.make_async_copy(ck, kb, lsem.at[0]),
         pltpu.make_async_copy(cv, vb, lsem.at[1]),
@@ -131,16 +141,21 @@
     barrier = pltpu.get_barrier_semaphore()
 
     def greet(k, carry):
-        other = (chip + k) % 64 * 2 + core
-        pl.semaphore_signal(barrier, inc=1, device_id=(other,), device_id_type=MESH)
+        mate = chip_of(group, (place + k) % 8) * 2 + core
+        counterpart = chip_of((group + k) % 8, place) * 2 + core
+        pl.semaphore_signal(barrier, inc=1, device_id=(mate,), device_id_type=MESH)
+        pl.semaphore_signal(barrier, inc=1, device_id=(counterpart,), device_id_type=MESH)
         return carry
 
+    for c in fetch:
+        c.start()
     pl.semaphore_signal(barrier, inc=1, device_id=(pair,), device_id_type=MESH)
-    lax.fori_loop(1, 64, greet, 0)
+    lax.fori_loop(1, 8, greet, 0, unroll=7)
     for c in local:
         c.start()
-    lax.fori_loop(0, 64, load_experts, 0)
-
+
+    for c in fetch:
+        c.wait()
     x = tok[...].astype(F32)
     normed = (x * lax.rsqrt(jnp.mean(x * x, axis=-1, keepdims=True) + EPS) * g1[...]).astype(BF)
     xa[place] = normed
@@ -159,7 +174,7 @@
     cs0[...] = shared
     cb[place] = shared
 
-    pl.semaphore_wait(barrier, 64)
+    pl.semaphore_wait(barrier, 15)
 
     def spread_strip(strip, buf, sems):
         slot = buf.at[group, core]
@@ -199,6 +214,7 @@
     in_group(lambda p: cs0, cb.at[place], s_cb)
     spread_strip(wo, wob, s_wo)
 
+    lax.fori_loop(0, 64, load_experts, 0, unroll=4)
     moved = to_block_order(tiles_of(tok[...].astype(F32)))
     for k in range(8):
         ts[k] = jnp.concatenate(moved[2 * k : 2 * k + 2], axis=1).astype(BF)
@@ -460,6 +476,14 @@
     take(zr.at[pl.ds(0, 63)], s_z.at[0])
 
 
+def write_out(a, b, c, a_out, b_out, c_out, sems):
+    copies = [pltpu.make_async_copy(src, dst, sems.at[k]) for k, (src, dst) in enumerate(((a, a_out), (b, b_out), (c, c_out)))]
+    for x in copies:
+        x.start()
+    for x in copies:
+        x.wait()
+
+
 def shards(
     tokens, cache_keys, cache_values, cache_len, norm_gain_first, w_query, w_key, w_value, head_bias,
     w_output, norm_gain_second, group_id, member, group_gate, member_weight, expert_gate_w, expert_up_w,
@@ -467,34 +491,33 @@
 ):
     vmem = pl.BlockSpec(memory_space=pltpu.VMEM)
     hbm = pl.BlockSpec(memory_space=pl.ANY)
-    smem = pl.BlockSpec(memory_space=pltpu.SMEM)
     V = pltpu.VMEM
     strips = (8, 2, SEQ, D)
     pair_sem = pltpu.SemaphoreType.DMA((2,))
     args = (
-        (tokens, vmem),
+        (tokens, hbm),
         (cache_keys, hbm),
         (cache_values, hbm),
-        (cache_len, smem),
-        (norm_gain_first.reshape(1, D), vmem),
-        (w_query.T, vmem),
+        (cache_len, hbm),
+        (norm_gain_first.reshape(1, D), hbm),
+        (w_query.T, hbm),
         (w_key, hbm),
         (w_value, hbm),
-        (head_bias.reshape(1, HEADS), vmem),
-        (w_output.T, vmem),
-        (norm_gain_second.reshape(1, D), vmem),
-        (group_id.reshape(1, SEQ), vmem),
-        (member.T, vmem),
-        (group_gate.reshape(1, SEQ), vmem),
-        (member_weight.T, vmem),
+        (head_bias.reshape(1, HEADS), hbm),
+        (w_output.T, hbm),
+        (norm_gain_second.reshape(1, D), hbm),
+        (group_id.reshape(1, SEQ), hbm),
+        (member.T, hbm),
+        (group_gate.reshape(1, SEQ), hbm),
+        (member_weight.T, hbm),
         (expert_gate_w, hbm),
         (expert_up_w, hbm),
         (expert_down_w, hbm),
-        (dense_gate_w.T, vmem),
-        (dense_up_w.T, vmem),
-        (hidden_gain.reshape(1, D), vmem),
-        (dense_down_w.T, vmem),
-        (branch_logit.reshape(1, D), vmem),
+        (dense_gate_w.T, hbm),
+        (dense_up_w.T, hbm),
+        (hidden_gain.reshape(1, D), hbm),
+        (dense_down_w.T, hbm),
+        (branch_logit.reshape(1, D), hbm),
     )
     scratch = [
         V((SEQ, CACHE, 128), BF),
@@ -551,13 +574,20 @@
         pltpu.SemaphoreType.DMA((6, 2)),
         pltpu.SemaphoreType.DMA((3, 2)),
     ] + [pair_sem] * 12
-    return pl.pallas_call(
+    for a, space in (
+        (0, V), (3, pltpu.SMEM), (4, V), (5, V), (8, V), (9, V), (10, V), (11, V),
+        (12, V), (13, V), (14, V), (18, V), (19, V), (20, V), (21, V), (22, V),
+    ):
+        scratch.append(space(args[a][0].shape, args[a][0].dtype))
+    scratch.append(pltpu.SemaphoreType.DMA((16,)))
+    shapes = (
+        jax.ShapeDtypeStruct((SEQ, D), BF),
+        jax.ShapeDtypeStruct((SEQ, 128), BF),
+        jax.ShapeDtypeStruct((SEQ, 128), BF),
+    )
+    made = pl.pallas_call(
         kernel,
-        out_shape=(
-            jax.ShapeDtypeStruct((SEQ, D), BF),
-            jax.ShapeDtypeStruct((SEQ, 128), BF),
-            jax.ShapeDtypeStruct((SEQ, 128), BF),
-        ),
+        out_shape=tuple(pltpu.VMEM(x.shape, x.dtype) for x in shapes),
         in_specs=[spec for _, spec in args],
         out_specs=(vmem, vmem, vmem),
         scratch_shapes=scratch,
@@ -565,6 +595,10 @@
             collective_id=0, has_side_effects=True, vmem_limit_bytes=62_000_000
         ),
     )(*[a for a, _ in args])
+    return pl.pallas_call(
+        write_out, out_shape=shapes, in_specs=[vmem] * 3, out_specs=(hbm,) * 3,
+        scratch_shapes=[pltpu.SemaphoreType.DMA((3,))],
+    )(*[pltpu.with_memory_space_constraint(x, pltpu.VMEM) for x in made])
 
 
 def solution(mesh):

time: 69.9 us -> 64.2 us (0.918)
  local copies, waits for them, and re-layouts: 4.02 us -> 0 us
  Pallas kernels: 64.9 us -> 62.8 us
    unnamed x3 -> x0, local copies, waits for them, and re-layouts: 4.02 us -> none
    pallas_call x1 -> x2, Pallas kernels: 64.9 us -> 62.8 us  [the longest x1 62.1 us: shards(): pl.pallas_call(kernel, out_shape=tuple((pltpu.VMEM(x.shape, x.dtype) for...]
where the time goes in v4:
time: 64.2 us; the launch traced here: 63.4 us
  Pallas kernels  62.8 us (98%)
  between operations  0.65 us (1%)
    pallas_call x1, Pallas kernels, shards(): pl.pallas_call(kernel, out_shape=tuple((pltpu.VMEM(x.shape, x.dtype) for...  62.1 us

profile of v4, /device:TPU:0, one launch (start us, length us, event | category | flops | bytes accessed | tf_op | source)
XLA Modules:
  0.0 63.4 jit_solution(7612466882009062933)
XLA Ops:
  0.6 62.1 %shard_map.238 = (bf16[16,2048]{1,0:T(8,128)(2,1)S(1)}, bf16[16,128]{1,0:T(8,128)(2,1)S(1)}, bf16[16,128]{1,0:T(8,128)(2,1)S(1)}) custom-call(bf16[16,2048]{1,0:T(8,128)(2,1)} %tok_h.1, bf16[16,1024,128]{2,1,0:T(8,128)(2,1)} %ck.1, bf16[16,1024,128]{2,1,0:T(8,128)(2,1)} %cv.1, s32[16]{0:T(128)} %clen_h.1, f32[1,2048]{1,0:T(1,128)} %bitcast.19, ...), custom_call_target="tpu_custom_call" | custom-call | tf_op jit(solution)/shard_map/pallas_call | solution.py:588
  62.8 0.7 %shard_map.239 = (bf16[16,2048]{1,0:T(8,128)(2,1)}, bf16[16,128]{1,0:T(8,128)(2,1)}, bf16[16,128]{1,0:T(8,128)(2,1)}) custom-call(bf16[16,2048]{1,0:T(8,128)(2,1)S(1)} %get-tuple-element.6.a, bf16[16,128]{1,0:T(8,128)(2,1)S(1)} %get-tuple-element.7.b, bf16[16,128]{1,0:T(8,128)(2,1)S(1)} %get-tuple-element.8.c), custom_call_target="tpu_custom_call" | custom-call | tf_op jit(solution)/shard_map/pallas_call | solution.py:598

commit v5 on v4

--- a/solution.py
+++ b/solution.py
@@ -103,7 +103,7 @@
     kb, vb, egb, eub, edb, wkb, wvb,
     wqb, wob, wgb, wub, wdb,
     xa, xc, xd, qs, qr, ts, tb, cs0, cb, cs, cd, pq, po, qstack, qb, ob, ps, pr, ys,
-    sq, sqr, zb, zs, zr, hbuf, zf, sc, wt, g2b, hgb, wgp, wup, wdp,
+    sq, sqr, zb, zs, zr, hbuf, zf, zd, wot, sc, wt, g2b, hgb, wgp, wup, wdp,
     lsem, s_wq, s_wo, s_wg, s_wu, s_wd, s_pair, s_ex, s_xa, s_xc, s_ts, s_cb, s_cd, s_q, s_pr, s_y, s_sq, s_z, s_wq2, s_xc2,
     tok, clen, g1, wq, hb, wo, g2, gid, mem, gg, mw, wg, wu, hg, wd, bl, fsem,
 ):
@@ -176,6 +176,8 @@
 
     pl.semaphore_wait(barrier, 15)
 
+    near, far = pl.ds(0, D // 2), pl.ds(D // 2, D // 2)
+
     def spread_strip(strip, buf, sems):
         slot = buf.at[group, core]
 
@@ -190,6 +192,45 @@
     def pass_on(buf, sems, k):
         take(buf.at[:, core], sems.at[1])
         remote(buf.at[:, core], buf.at[:, core], s_pair.at[k], pair).start()
+
+    depth, side = group // 2, group % 2
+    mirror = chip_of(group + 1 - 2 * side, place) * 2 + core
+
+    def along_z(src, dst, sem):
+        def send(k, carry):
+            remote(src, dst, sem, chip_of((depth + k) % 4 * 2 + side, place) * 2 + core).start()
+            return carry
+
+        lax.fori_loop(1, 4, send, 0)
+
+    def plant(strip, buf, sems):
+        slot = buf.at[depth, side, core]
+        pltpu.make_async_copy(strip, slot, sems.at[5, 1]).start()
+        along_z(strip.at[:, near], slot.at[:, near], sems.at[0])
+        remote(strip.at[:, far], slot.at[:, far], sems.at[1], mirror).start()
+        along_z(strip.at[:, far], slot.at[:, far], sems.at[2])
+
+    def relay(buf, sems):
+        take(buf.at[0, 0, core], sems.at[5, 1])
+        take(buf.at[0, 0, core, :, far], sems.at[1, 1])
+        ahead = buf.at[depth, 1 - side, core, :, far]
+        along_z(ahead, ahead, sems.at[3])
+        take(buf.at[pl.ds(0, 3), 0, core, :, near], sems.at[0, 1])
+        across = buf.at[:, side, core, :, near]
+        remote(across, across, sems.at[4], mirror).start()
+
+    def finish(buf, sems, k):
+        take(buf.at[pl.ds(0, 3), 0, core, :, far], sems.at[2, 1])
+        take(buf.at[pl.ds(0, 3), 0, core, :, far], sems.at[3, 1])
+        take(buf.at[:, 0, core, :, near], sems.at[4, 1])
+        remote(buf.at[:, :, core], buf.at[:, :, core], s_pair.at[k], pair).start()
+
+    def uproot(buf, sems):
+        take(buf.at[pl.ds(0, 3), 0, core, :, near], sems.at[0, 0])
+        take(buf.at[0, 0, core, :, far], sems.at[1, 0])
+        take(buf.at[pl.ds(0, 3), 0, core, :, far], sems.at[2, 0])
+        take(buf.at[pl.ds(0, 3), 0, core, :, far], sems.at[3, 0])
+        take(buf.at[:, 0, core, :, near], sems.at[4, 0])
 
     def in_group(src_of, dst, sems):
         def send(k, carry):
@@ -201,18 +242,20 @@
 
     def over_plane(src_of, dst_of, sems):
         def send(k, carry):
-            other = (chip + k) % 64
+            other = (chip + k * 27) % 64
             remote(src_of(other), dst_of(other), sems, other * 2 + core).start()
             return carry
 
         lax.fori_loop(1, 64, send, 0, unroll=7)
 
-    near, far = pl.ds(0, D // 2), pl.ds(D // 2, D // 2)
     spread_strip(wq.at[:, near], wqb.at[:, :, :, near], s_wq)
     spread_strip(wq.at[:, far], wqb.at[:, :, :, far], s_wq2)
     in_group(lambda p: xa.at[place], xa.at[place], s_xa)
     in_group(lambda p: cs0, cb.at[place], s_cb)
-    spread_strip(wo, wob, s_wo)
+
+    @pl.when(core == 0)
+    def _():
+        plant(wo, wob, s_wo)
 
     lax.fori_loop(0, 64, load_experts, 0, unroll=4)
     moved = to_block_order(tiles_of(tok[...].astype(F32)))
@@ -223,8 +266,12 @@
     for src, dst in ((g2, g2b), (hg, hgb), (wg, wgp), (wu, wup), (wd, wdp)):
         for k, tile in enumerate(to_block_order(tiles_of(src[...].astype(F32)))):
             dst[:, k * 128 : (k + 1) * 128] = tile.astype(dst.dtype)
-    spread_strip(wgp, wgb, s_wg)
-    spread_strip(wup, wub, s_wu)
+
+    @pl.when(core == 0)
+    def _():
+        plant(wgp, wgb, s_wg)
+        plant(wup, wub, s_wu)
+
     local[2].wait()
     local[3].wait()
     nk[...] = dot(normed, wkb[...]).astype(BF)
@@ -242,6 +289,13 @@
 
     pass_on(wqb.at[:, :, :, near], s_wq, 0)
     pass_on(wqb.at[:, :, :, far], s_wq2, 5)
+
+    @pl.when(core == 1)
+    def _():
+        plant(wo, wob, s_wo)
+        plant(wgp, wgb, s_wg)
+        plant(wup, wub, s_wu)
+
     take(xa.at[pl.ds(0, 7)], s_xa.at[1])
     take(wqb.at[:, core, :, near], s_pair.at[0, 1])
     q = dot_nt(xa[:, :, : D // 2].reshape(128, D // 2), wqb[:, :, :, : D // 2].reshape(BLK, D // 2))
@@ -274,6 +328,7 @@
 
     lax.fori_loop(1, 8, send_comb, 0)
 
+    relay(wob, s_wo)
     over_plane(lambda o: wdp.at[:, lanes((o % 8 // 4 + o // 8) % 2 * 4 + o % 4)], lambda o: wdb.at[chip, core], s_wd)
     own_wd = pltpu.make_async_copy(wdp.at[:, lanes(place)], wdb.at[chip, core], lsem.at[7])
     own_wd.start()
@@ -343,13 +398,16 @@
             mix(t - 2)
         if t == 5:
             hand_out(0)
-            pass_on(wob, s_wo, 1)
     hand_out(1)
-
-    take(wob.at[:, core], s_pair.at[1, 1])
+    relay(wgb, s_wg)
+    finish(wob, s_wo, 1)
+    relay(wub, s_wu)
+
+    take(wob.at[:, :, core], s_pair.at[1, 1])
+    wot[...] = wob[...].reshape(BLK, D).T
     take(xc.at[pl.ds(0, 7), pl.ds(0, 8)], s_xc.at[1])
     take(xc.at[pl.ds(0, 7), pl.ds(0, 8)], s_xc2.at[1])
-    proj = dot_nt(xc[...].reshape(128, D), wob[...].reshape(BLK, D)).astype(BF)
+    proj = dot(xc[...].reshape(128, D), wot[...]).astype(BF)
     stream = tb[...].reshape(128, BLK).astype(F32) + proj.astype(F32)
     y = (stream * g2b[:, lanes(place)]).astype(BF)
     ys[...] = dot(regroup_bf, y).astype(BF).reshape(8, SEQ, BLK)
@@ -359,8 +417,8 @@
     pr[:, lanes(place)] = ps[place]
     in_group(lambda p: ps.at[p], pr.at[:, lanes(place)], s_pr)
 
-    pass_on(wgb, s_wg, 2)
-    pass_on(wub, s_wu, 3)
+    finish(wgb, s_wg, 2)
+    finish(wub, s_wu, 3)
     own_wd.wait()
     take(wdb.at[pl.ds(0, 63), core], s_wd.at[1])
     remote(wdb.at[:, core], wdb.at[:, core], s_pair.at[4], pair).start()
@@ -376,8 +434,8 @@
     rows_in = xd[...].reshape(128, D)
     plain = rows_in.astype(F32) * (1.0 / g2b[...])
     scale = lax.rsqrt(jnp.mean(plain * plain, axis=1, keepdims=True) + EPS)
-    take(wgb.at[:, core], s_pair.at[2, 1])
-    take(wub.at[:, core], s_pair.at[3, 1])
+    take(wgb.at[:, :, core], s_pair.at[2, 1])
+    take(wub.at[:, :, core], s_pair.at[3, 1])
     gate = dot_nt(rows_in, wgb[...].reshape(BLK, D)) * scale
     upper = dot_nt(rows_in, wub[...].reshape(BLK, D)) * scale
     hidden = gate * jax.nn.sigmoid(gate) * upper
@@ -401,48 +459,54 @@
         return carry
 
     lax.fori_loop(0, 8, route, 0, unroll=2)
-    take(sqr.at[pl.ds(0, 7)], s_sq.at[1])
-    total = jnp.sum(sqr[...], axis=0)[0:1, :]
-    total_col = jnp.sum(jnp.where(eye, jnp.broadcast_to(total, (128, 128)), 0.0), axis=1, keepdims=True)
-    dense_scale = lax.rsqrt(total_col * (1.0 / D) + EPS)
-    dense = (hidden * dense_scale * hgb[:, lanes(place)]).astype(BF)
+    dense = (hidden * hgb[:, lanes(place)]).astype(BF)
     take(wdb.at[:, core], s_pair.at[4, 1])
 
-    def produce(k, carry):
-        down = dot_nt(dense, wdb[pl.ds(k * 8, 8)].reshape(BLK, BLK))
-        z = zf[:, lanes(k)] + jax.nn.sigmoid(bl[:, lanes(k)]) * down
-        zb[k] = z.astype(BF).reshape(8, SEQ, BLK)
+    def down(k, carry):
+        v = dot_nt(dense, wdb[pl.ds(k * 8, 8)].reshape(BLK, BLK))
+        zd[:, lanes(k)] = jax.nn.sigmoid(bl[:, lanes(k)]) * v
         return carry
 
-    lax.fori_loop(0, 8, produce, 0, unroll=2)
-
-    def give(k, carry):
-        g = (group + k) % 8
-        zs[g] = dot(fold, zb[:, g].reshape(128, BLK)).astype(BF).reshape(8, SEQ, BLK)
-
-        def send(j, carry):
-            p = (place + j) % 8
-            remote(zs.at[g, p], zr.at[chip], s_z, chip_of(g, p) * 2 + core).start()
-            return carry
-
-        @pl.when(g == group)
-        def _():
-            zr[chip] = zs[g, place]
-
-        @pl.when(g != group)
-        def _():
-            send(0, 0)
-
-        lax.fori_loop(1, 8, send, 0)
-        return carry
-
-    lax.fori_loop(0, 8, give, 0)
-
+    lax.fori_loop(0, 8, down, 0, unroll=2)
     spots = dot_nt(one_hot(iota((128, SEQ), 0) % 16 == iota((128, SEQ), 1)), order)
     unfold = dot(spots, one_hot(iota((SEQ, 128), 1) // 8 == iota((SEQ, 128), 0)))
     unfold = jnp.where(r // 16 == c % 8, unfold, 0.0).astype(BF)
     take(pr.at[:, pl.ds(0, 7 * BLK)], s_pr.at[1])
     second = from_block_order(tiles_of(pr[...].astype(F32)))
+    take(sqr.at[pl.ds(0, 7)], s_sq.at[1])
+    total = jnp.sum(sqr[...], axis=0)[0:1, :]
+    total_col = jnp.sum(jnp.where(eye, jnp.broadcast_to(total, (128, 128)), 0.0), axis=1, keepdims=True)
+    dense_scale = lax.rsqrt(total_col * (1.0 / D) + EPS)
+
+    def produce(k, carry):
+        z = zf[:, lanes(k)] + dense_scale * zd[:, lanes(k)]
+        zb[k] = z.astype(BF).reshape(8, SEQ, BLK)
+        return carry
+
+    lax.fori_loop(0, 8, produce, 0, unroll=2)
+
+    def give(k, carry):
+        g = (group + k) % 8
+        zs[g] = dot(fold, zb[:, g].reshape(128, BLK)).astype(BF).reshape(8, SEQ, BLK)
+
+        def send(j, carry):
+            p = (place + j) % 8
+            remote(zs.at[g, p], zr.at[chip], s_z, chip_of(g, p) * 2 + core).start()
+            return carry
+
+        @pl.when(g == group)
+        def _():
+            zr[chip] = zs[g, place]
+
+        @pl.when(g != group)
+        def _():
+            send(0, 0)
+
+        lax.fori_loop(1, 8, send, 0)
+        return carry
+
+    lax.fori_loop(0, 8, give, 0)
+
     take(zr.at[pl.ds(0, 63)], s_z.at[1])
     sums = jnp.sum(zr[...].reshape(8, 8, SEQ, BLK).astype(F32), axis=1).reshape(128, BLK)
     high, low = split2(sums)
@@ -454,11 +518,13 @@
 
     take(wqb.at[pl.ds(0, 7), core, :, near], s_wq.at[0])
     take(wqb.at[pl.ds(0, 7), core, :, far], s_wq2.at[0])
-    take(wob.at[pl.ds(0, 7), core], s_wo.at[0])
-    take(wgb.at[pl.ds(0, 7), core], s_wg.at[0])
-    take(wub.at[pl.ds(0, 7), core], s_wu.at[0])
+    uproot(wob, s_wo)
+    uproot(wgb, s_wg)
+    uproot(wub, s_wu)
     take(wdb.at[pl.ds(0, 63), core], s_wd.at[0])
-    for k, buf in enumerate((wqb.at[:, :, :, near], wob, wgb, wub, wdb, wqb.at[:, :, :, far])):
+    for k, buf in enumerate((wob, wgb, wub)):
+        take(buf.at[:, :, core], s_pair.at[k + 1, 0])
+    for k, buf in ((0, wqb.at[:, :, :, near]), (4, wdb), (5, wqb.at[:, :, :, far])):
         take(buf.at[:, core], s_pair.at[k, 0])
     take(edb.at[1], s_ex.at[0, 0])
     take(egb.at[1], s_ex.at[1, 0])
@@ -494,6 +560,7 @@
     V = pltpu.VMEM
     strips = (8, 2, SEQ, D)
     pair_sem = pltpu.SemaphoreType.DMA((2,))
+    tree_sem = pltpu.SemaphoreType.DMA((6, 2))
     args = (
         (tokens, hbm),
         (cache_keys, hbm),
@@ -528,9 +595,9 @@
         V((D, 128), BF),
         V((D, 128), BF),
         V(strips, BF),
-        V(strips, BF),
-        V(strips, BF),
-        V(strips, BF),
+        V((4, 2, 2, SEQ, D), BF),
+        V((4, 2, 2, SEQ, D), BF),
+        V((4, 2, 2, SEQ, D), BF),
         V((64, 2, SEQ, BLK), BF),
         V((8, SEQ, D), BF),
         V((8, SEQ, D), BF),
@@ -558,6 +625,8 @@
         V((64, SEQ, BLK), BF),
         V((128, 1024), BF),
         V((128, D), F32),
+        V((128, D), F32),
+        V((D, BLK), BF),
         V((2, 2, HEADS, CACHE), F32),
         V((2, 2, HEADS, CACHE), BF),
         V((1, D), F32),
@@ -567,9 +636,9 @@
         V((SEQ, D), BF),
         pltpu.SemaphoreType.DMA((8,)),
         pair_sem,
-        pair_sem,
-        pair_sem,
-        pair_sem,
+        tree_sem,
+        tree_sem,
+        tree_sem,
         pair_sem,
         pltpu.SemaphoreType.DMA((6, 2)),
         pltpu.SemaphoreType.DMA((3, 2)),

time: 64.2 us -> 61.2 us (0.953)
  Pallas kernels: 62.8 us -> 59.7 us
    pallas_call x1, Pallas kernels: 62.1 us -> 59 us  [shards(): pl.pallas_call(kernel, out_shape=tuple((pltpu.VMEM(x.shape, x.dtype) for...]
where the time goes in v5:
time: 61.2 us; the launch traced here: 60.3 us
  Pallas kernels  59.7 us (98%)
  between operations  0.65 us (1%)
    pallas_call x1, Pallas kernels, shards(): pl.pallas_call(kernel, out_shape=tuple((pltpu.VMEM(x.shape, x.dtype) for...  59 us

profile of v5, /device:TPU:0, one launch (start us, length us, event | category | flops | bytes accessed | tf_op | source)
XLA Modules:
  0.0 60.3 jit_solution(1513029091165229919)
XLA Ops:
  0.6 59.0 %shard_map.238 = (bf16[16,2048]{1,0:T(8,128)(2,1)S(1)}, bf16[16,128]{1,0:T(8,128)(2,1)S(1)}, bf16[16,128]{1,0:T(8,128)(2,1)S(1)}) custom-call(bf16[16,2048]{1,0:T(8,128)(2,1)} %tok_h.1, bf16[16,1024,128]{2,1,0:T(8,128)(2,1)} %ck.1, bf16[16,1024,128]{2,1,0:T(8,128)(2,1)} %cv.1, s32[16]{0:T(128)} %clen_h.1, f32[1,2048]{1,0:T(1,128)} %bitcast.19, ...), custom_call_target="tpu_custom_call" | custom-call | tf_op jit(solution)/shard_map/pallas_call | solution.py:657
  59.6 0.7 %shard_map.239 = (bf16[16,2048]{1,0:T(8,128)(2,1)}, bf16[16,128]{1,0:T(8,128)(2,1)}, bf16[16,128]{1,0:T(8,128)(2,1)}) custom-call(bf16[16,2048]{1,0:T(8,128)(2,1)S(1)} %get-tuple-element.6.a, bf16[16,128]{1,0:T(8,128)(2,1)S(1)} %get-tuple-element.7.b, bf16[16,128]{1,0:T(8,128)(2,1)S(1)} %get-tuple-element.8.c), custom_call_target="tpu_custom_call" | custom-call | tf_op jit(solution)/shard_map/pallas_call | solution.py:667

commit v6 on v5

--- a/solution.py
+++ b/solution.py
@@ -103,7 +103,7 @@
     kb, vb, egb, eub, edb, wkb, wvb,
     wqb, wob, wgb, wub, wdb,
     xa, xc, xd, qs, qr, ts, tb, cs0, cb, cs, cd, pq, po, qstack, qb, ob, ps, pr, ys,
-    sq, sqr, zb, zs, zr, hbuf, zf, zd, wot, sc, wt, g2b, hgb, wgp, wup, wdp,
+    sq, sqr, zb, zs, zr, hbuf, zf, zd, wot, wgt, wut, sc, wt, g2b, hgb, wgp, wup, wdp,
     lsem, s_wq, s_wo, s_wg, s_wu, s_wd, s_pair, s_ex, s_xa, s_xc, s_ts, s_cb, s_cd, s_q, s_pr, s_y, s_sq, s_z, s_wq2, s_xc2,
     tok, clen, g1, wq, hb, wo, g2, gid, mem, gg, mw, wg, wu, hg, wd, bl, fsem,
 ):
@@ -270,7 +270,6 @@
     @pl.when(core == 0)
     def _():
         plant(wgp, wgb, s_wg)
-        plant(wup, wub, s_wu)
 
     local[2].wait()
     local[3].wait()
@@ -294,7 +293,6 @@
     def _():
         plant(wo, wob, s_wo)
         plant(wgp, wgb, s_wg)
-        plant(wup, wub, s_wu)
 
     take(xa.at[pl.ds(0, 7)], s_xa.at[1])
     take(wqb.at[:, core, :, near], s_pair.at[0, 1])
@@ -329,18 +327,24 @@
     lax.fori_loop(1, 8, send_comb, 0)
 
     relay(wob, s_wo)
+    plant(wup, wub, s_wu)
     over_plane(lambda o: wdp.at[:, lanes((o % 8 // 4 + o // 8) % 2 * 4 + o % 4)], lambda o: wdb.at[chip, core], s_wd)
     own_wd = pltpu.make_async_copy(wdp.at[:, lanes(place)], wdb.at[chip, core], lsem.at[7])
     own_wd.start()
 
     take(qr.at[:, pl.ds(0, 7 * BLK)], s_q.at[1])
-    left = iota((SEQ, 128), 1) < HEAD_DIM
-    for t, v in enumerate(from_block_order(tiles_of(qr[...].astype(F32) * HEAD_DIM**-0.5))):
-        w = pltpu.roll(v, HEAD_DIM, 1)
-        first, second = (v, w) if t < 8 else (w, v)
-        keep = left if t < 8 else jnp.logical_not(left)
-        qstack[32 * t : 32 * t + 16, :] = jnp.where(keep, first, 0.0).astype(BF)
-        qstack[32 * t + 16 : 32 * t + 32, :] = jnp.where(keep, second, 0.0).astype(BF)
+    came = tiles_of(qr[...].astype(F32) * HEAD_DIM**-0.5)
+    quarter = iota((SEQ, 128), 1) // 32
+    for h in range(HEADS):
+        t, g, yl = h // 2, h // 4, h // 2 % 2
+        row = jnp.zeros((SEQ, 128), F32)
+        for k in range(2):
+            p = (yl + g) % 2 * 4 + h % 2 * 2 + k
+            at = (2 if t >= 8 else 0) + k
+            shift = (at - g % 4) * 32 % 128
+            v = came[p * 2 + g // 4]
+            row = jnp.where(quarter == at, pltpu.roll(v, shift, 1) if shift else v, row)
+        qstack[16 * h : 16 * h + 16, :] = row.astype(BF)
     qb[...] = dot(pq[...], qstack[...]).astype(BF).reshape(SEQ, HEADS, 128)
     local[0].wait()
     local[1].wait()
@@ -430,14 +434,17 @@
     comb0 = jnp.sum(jnp.where(lane == member0, comb, 0.0), axis=1, keepdims=True)
     comb1 = jnp.sum(jnp.where(lane == member1, comb, 0.0), axis=1, keepdims=True)
 
+    take(wgb.at[:, :, core], s_pair.at[2, 1])
+    wgt[...] = wgb[...].reshape(BLK, D).T
+    take(wub.at[:, :, core], s_pair.at[3, 1])
+    wut[...] = wub[...].reshape(BLK, D).T
+
     take(zr.at[pl.ds(0, 63)], s_y.at[1])
     rows_in = xd[...].reshape(128, D)
     plain = rows_in.astype(F32) * (1.0 / g2b[...])
     scale = lax.rsqrt(jnp.mean(plain * plain, axis=1, keepdims=True) + EPS)
-    take(wgb.at[:, :, core], s_pair.at[2, 1])
-    take(wub.at[:, :, core], s_pair.at[3, 1])
-    gate = dot_nt(rows_in, wgb[...].reshape(BLK, D)) * scale
-    upper = dot_nt(rows_in, wub[...].reshape(BLK, D)) * scale
+    gate = dot(rows_in, wgt[...]) * scale
+    upper = dot(rows_in, wut[...]) * scale
     hidden = gate * jax.nn.sigmoid(gate) * upper
     part = jnp.sum(hidden * hidden, axis=1, keepdims=True)
     part_row = jnp.sum(jnp.where(eye, jnp.broadcast_to(part, (128, 128)), 0.0), axis=0, keepdims=True)
@@ -627,6 +634,8 @@
         V((128, D), F32),
         V((128, D), F32),
         V((D, BLK), BF),
+        V((D, BLK), BF),
+        V((D, BLK), BF),
         V((2, 2, HEADS, CACHE), F32),
         V((2, 2, HEADS, CACHE), BF),
         V((1, D), F32),

time: 61.2 us -> 60.9 us (level)
  no operation moved by 1% of the time
where the time goes in v6:
time: 60.9 us; the launch traced here: 60.1 us
  Pallas kernels  59.5 us (98%)
  between operations  0.65 us (1%)
    pallas_call x1, Pallas kernels, shards(): pl.pallas_call(kernel, out_shape=tuple((pltpu.VMEM(x.shape, x.dtype) for...  58.8 us

profile of v6, /device:TPU:0, one launch (start us, length us, event | category | flops | bytes accessed | tf_op | source)
XLA Modules:
  0.0 60.1 jit_solution(6785337911144313918)
XLA Ops:
  0.6 58.8 %shard_map.238 = (bf16[16,2048]{1,0:T(8,128)(2,1)S(1)}, bf16[16,128]{1,0:T(8,128)(2,1)S(1)}, bf16[16,128]{1,0:T(8,128)(2,1)S(1)}) custom-call(bf16[16,2048]{1,0:T(8,128)(2,1)} %tok_h.1, bf16[16,1024,128]{2,1,0:T(8,128)(2,1)} %ck.1, bf16[16,1024,128]{2,1,0:T(8,128)(2,1)} %cv.1, s32[16]{0:T(128)} %clen_h.1, f32[1,2048]{1,0:T(1,128)} %bitcast.19, ...), custom_call_target="tpu_custom_call" | custom-call | tf_op jit(solution)/shard_map/pallas_call | solution.py:666
  59.4 0.7 %shard_map.239 = (bf16[16,2048]{1,0:T(8,128)(2,1)}, bf16[16,128]{1,0:T(8,128)(2,1)}, bf16[16,128]{1,0:T(8,128)(2,1)}) custom-call(bf16[16,2048]{1,0:T(8,128)(2,1)S(1)} %get-tuple-element.6.a, bf16[16,128]{1,0:T(8,128)(2,1)S(1)} %get-tuple-element.7.b, bf16[16,128]{1,0:T(8,128)(2,1)S(1)} %get-tuple-element.8.c), custom_call_target="tpu_custom_call" | custom-call | tf_op jit(solution)/shard_map/pallas_call | solution.py:676

commit v7 on v6

--- a/solution.py
+++ b/solution.py
@@ -181,13 +181,10 @@
     def spread_strip(strip, buf, sems):
         slot = buf.at[group, core]
 
-        def send(k, carry):
-            g = (group + k) % 8
+        pltpu.make_async_copy(strip, slot, sems.at[1]).start()
+        for dz, dh in ((2, 1), (2, 0), (1, 1), (3, 1), (1, 0), (3, 0), (0, 1)):
+            g = (group // 2 + dz) % 4 * 2 + (group + dh) % 2
             remote(strip, slot, sems, chip_of(g, place) * 2 + core).start()
-            return carry
-
-        pltpu.make_async_copy(strip, slot, sems.at[1]).start()
-        lax.fori_loop(1, 8, send, 0)
 
     def pass_on(buf, sems, k):
         take(buf.at[:, core], sems.at[1])
@@ -197,11 +194,8 @@
     mirror = chip_of(group + 1 - 2 * side, place) * 2 + core
 
     def along_z(src, dst, sem):
-        def send(k, carry):
+        for k in (2, 1, 3):
             remote(src, dst, sem, chip_of((depth + k) % 4 * 2 + side, place) * 2 + core).start()
-            return carry
-
-        lax.fori_loop(1, 4, send, 0)
 
     def plant(strip, buf, sems):
         slot = buf.at[depth, side, core]
@@ -233,20 +227,31 @@
         take(buf.at[:, 0, core, :, near], sems.at[4, 0])
 
     def in_group(src_of, dst, sems):
-        def send(k, carry):
-            p = (place + k) % 8
+        for dy, dx in ((1, 2), (0, 2), (1, 1), (1, 3), (0, 1), (0, 3), (1, 0)):
+            p = (place // 4 + dy) % 2 * 4 + (place + dx) % 4
             remote(src_of(p), dst, sems, chip_of(group, p) * 2 + core).start()
+
+    def over_plane(src_of, dst_of, sems):
+        def one(dz, dy, dx):
+            other = (depth + dz) % 4 * 16 + (chip // 4 + dy) % 4 * 4 + (chip + dx) % 4
+            remote(src_of(other), dst_of(other), sems, other * 2 + core).start()
+
+        def far_plane(k, carry):
+            m = k * 7 % 16
+            one(2, m // 4 + 2, m % 4 + 2)
             return carry
 
-        lax.fori_loop(1, 8, send, 0)
-
-    def over_plane(src_of, dst_of, sems):
-        def send(k, carry):
-            other = (chip + k * 27) % 64
-            remote(src_of(other), dst_of(other), sems, other * 2 + core).start()
+        def next_planes(k, carry):
+            m = k * 7 % 16
+            one(1, m // 4 + 2, m % 4 + 2)
+            one(3, m % 4 + 2, m // 4 + 2)
             return carry
 
-        lax.fori_loop(1, 64, send, 0, unroll=7)
+        lax.fori_loop(0, 16, far_plane, 0, unroll=4)
+        lax.fori_loop(0, 16, next_planes, 0, unroll=4)
+        own = [(y, x) for y in range(4) for x in range(4) if y or x]
+        for y, x in sorted(own, key=lambda v: -min(v[0], 4 - v[0]) - min(v[1], 4 - v[1])):
+            one(0, y, x)
 
     spread_strip(wq.at[:, near], wqb.at[:, :, :, near], s_wq)
     spread_strip(wq.at[:, far], wqb.at[:, :, :, far], s_wq2)
@@ -492,27 +497,23 @@
 
     lax.fori_loop(0, 8, produce, 0, unroll=2)
 
-    def give(k, carry):
-        g = (group + k) % 8
+    def give(dz, dh):
+        g = (depth + dz) % 4 * 2 + (side + dh) % 2
         zs[g] = dot(fold, zb[:, g].reshape(128, BLK)).astype(BF).reshape(8, SEQ, BLK)
 
         def send(j, carry):
-            p = (place + j) % 8
+            p = (place + j * 3 + dz) % 8 if dz or dh else (place + j * 3) % 8
             remote(zs.at[g, p], zr.at[chip], s_z, chip_of(g, p) * 2 + core).start()
             return carry
 
-        @pl.when(g == group)
-        def _():
+        if dz or dh:
+            lax.fori_loop(0, 8, send, 0)
+        else:
             zr[chip] = zs[g, place]
-
-        @pl.when(g != group)
-        def _():
-            send(0, 0)
-
-        lax.fori_loop(1, 8, send, 0)
-        return carry
-
-    lax.fori_loop(0, 8, give, 0)
+            lax.fori_loop(1, 8, send, 0)
+
+    for dz, dh in ((2, 1), (2, 0), (1, 1), (3, 1), (1, 0), (3, 0), (0, 1), (0, 0)):
+        give(dz, dh)
 
     take(zr.at[pl.ds(0, 63)], s_z.at[1])
     sums = jnp.sum(zr[...].reshape(8, 8, SEQ, BLK).astype(F32), axis=1).reshape(128, BLK)

time: 60.9 us -> 58.5 us (0.961)
  Pallas kernels: 59.5 us -> 57.5 us
    pallas_call x1, Pallas kernels: 58.8 us -> 56.8 us  [shards(): pl.pallas_call(kernel, out_shape=tuple((pltpu.VMEM(x.shape, x.dtype) for...]
where the time goes in v7:
time: 58.5 us; the launch traced here: 58.2 us
  Pallas kernels  57.5 us (98%)
  between operations  0.65 us (1%)
    pallas_call x1, Pallas kernels, shards(): pl.pallas_call(kernel, out_shape=tuple((pltpu.VMEM(x.shape, x.dtype) for...  56.8 us

profile of v7, /device:TPU:0, one launch (start us, length us, event | category | flops | bytes accessed | tf_op | source)
XLA Modules:
  0.0 58.2 jit_solution(15613042497222521419)
XLA Ops:
  0.6 56.8 %shard_map.238 = (bf16[16,2048]{1,0:T(8,128)(2,1)S(1)}, bf16[16,128]{1,0:T(8,128)(2,1)S(1)}, bf16[16,128]{1,0:T(8,128)(2,1)S(1)}) custom-call(bf16[16,2048]{1,0:T(8,128)(2,1)} %tok_h.1, bf16[16,1024,128]{2,1,0:T(8,128)(2,1)} %ck.1, bf16[16,1024,128]{2,1,0:T(8,128)(2,1)} %cv.1, s32[16]{0:T(128)} %clen_h.1, f32[1,2048]{1,0:T(1,128)} %bitcast.19, ...), custom_call_target="tpu_custom_call" | custom-call | tf_op jit(solution)/shard_map/pallas_call | solution.py:667
  57.5 0.7 %shard_map.239 = (bf16[16,2048]{1,0:T(8,128)(2,1)}, bf16[16,128]{1,0:T(8,128)(2,1)}, bf16[16,128]{1,0:T(8,128)(2,1)}) custom-call(bf16[16,2048]{1,0:T(8,128)(2,1)S(1)} %get-tuple-element.6.a, bf16[16,128]{1,0:T(8,128)(2,1)S(1)} %get-tuple-element.7.b, bf16[16,128]{1,0:T(8,128)(2,1)S(1)} %get-tuple-element.8.c), custom_call_target="tpu_custom_call" | custom-call | tf_op jit(solution)/shard_map/pallas_call | solution.py:677
